TPU v7x, 32 devices: a whole 2x2x4 slice. The times are simulated.
32 devices in a mesh: sp: 16 (over z, y, core), tp: 2 (over x).
Axes of the slice: x: 2, y: 2, z: 4, core: 2. Of those that a mesh axis runs over, the one named last changes fastest.
Arguments:
- resid: bfloat16 [8192, 2048], P(('sp', 'tp')), may hold values from -3 to 3
- queries: bfloat16 [8192, 1024], P('sp', 'tp'), may hold values from -6 to 6
- keys: bfloat16 [8192, 512], P('sp', 'tp'), may hold values from -6 to 6
- values: bfloat16 [8192, 512], P('sp', 'tp'), may hold values from -6 to 6
- documents: int32 [8192], P('sp'), may hold values from 0 to 7, never falling along the last dimension, each value on 1 to 2048 neighbouring positions
- sinks: float32 [16], P('tp'), may hold values from 0 to 5
- out_proj: bfloat16 [1024, 2048], replicated, may hold values from -0.75 to 0.75
- norm_gain: float32 [2048], replicated, may hold values from 0.1 to 1.9
- gate_proj: bfloat16 [2048, 5632], P('sp', 'tp'), may hold values from -0.125 to 0.125
- up_proj: bfloat16 [2048, 5632], P('sp', 'tp'), may hold values from -0.125 to 0.125
- down_proj: bfloat16 [5632, 2048], P('tp', 'sp'), may hold values from -0.078125 to 0.078125
Outputs:
- mixed: bfloat16 [8192, 2048], P(('sp', 'tp'))
Inputs may be any that keep to these rules, and one draw needn't show every extreme that they name: `documents`: document numbers never fall along the sequence; each document holds at most 2048 positions.
All inputs are finite; a program needn't handle non-finite values.
Results may differ from a plain program's by a relative error of at most 0.0095.
Values may be sent and summed in bfloat16 or wider, within the bound.
A program may use at most 128 MiB of HBM per device.

v0:
```python
import jax
import jax.numpy as jnp
from jax import lax
from jax.experimental import pallas as pl
from jax.experimental.pallas import tpu as pltpu
from jax.sharding import PartitionSpec as P

HD = 64
WINDOW = 128
SHARE = 4


def passed_along(value, axis, steps):
    count = lax.axis_size(axis)
    first, last = (max(0, -steps), min(count, count - steps))
    return lax.ppermute(value, axis, [(source, source + steps) for source in range(first, last)])


def swapped(value, axis, mask):
    count = lax.axis_size(axis)
    return lax.ppermute(value, axis, [(source, source ^ mask) for source in range(count)])


def bits_of(count):
    return [1 << bit for bit in range(count.bit_length() - 1)]


def attend(queries, keys, values, documents, sinks):
    rows = queries.shape[0]
    kv_heads = keys.shape[1] // HD
    group = queries.shape[1] // HD // kv_heads
    blocks = rows // WINDOW
    key_value = jnp.concatenate([keys, values], axis=1)
    tail_pair, tail_docs = passed_along(
        (key_value[rows - WINDOW :], documents[rows - WINDOW :].astype(jnp.bfloat16)), "sp", 1
    )
    ext_pair = jnp.concatenate([tail_pair, key_value], axis=0).reshape(
        blocks + 1, WINDOW, 2 * kv_heads * HD
    )
    ext_docs = jnp.concatenate([tail_docs.astype(jnp.int32), documents], axis=0).reshape(
        blocks + 1, WINDOW
    )
    band = jnp.concatenate([ext_pair[:-1], ext_pair[1:]], axis=1)
    band_keys = band[:, :, : kv_heads * HD].reshape(blocks, 2 * WINDOW, kv_heads, HD)
    band_values = band[:, :, kv_heads * HD :].reshape(blocks, 2 * WINDOW, kv_heads, HD)
    band_docs = jnp.concatenate([ext_docs[:-1], ext_docs[1:]], axis=1)
    query_docs = documents.reshape(blocks, WINDOW)
    offset = lax.axis_index("sp") * rows
    distance = jnp.arange(WINDOW)[:, None] + WINDOW - jnp.arange(2 * WINDOW)[None, :]
    key_pos = (
        offset + jnp.arange(blocks)[:, None] * WINDOW + jnp.arange(2 * WINDOW)[None, :] - WINDOW
    )
    visible = (
        ((distance >= 0) & (distance < WINDOW))[None]
        & (key_pos >= 0)[:, None, :]
        & (band_docs[:, None, :] == query_docs[:, :, None])
    )
    query_blocks = queries.reshape(blocks, WINDOW, kv_heads, group, HD)
    scores = jnp.einsum(
        "nikgd,njkd->nkgij", query_blocks, band_keys, preferred_element_type=jnp.float32
    ) * HD ** (-0.5)
    scores = jnp.where(visible[:, None, None], scores, -jnp.inf)
    sink_logit = sinks.reshape(kv_heads, group)[None, :, :, None, None]
    row_top = jnp.maximum(jnp.max(scores, axis=-1, keepdims=True), sink_logit)
    raw_weights = jnp.exp(scores - row_top)
    totals = jnp.sum(raw_weights, axis=-1, keepdims=True) + jnp.exp(sink_logit - row_top)
    weights = (raw_weights / totals).astype(jnp.bfloat16)
    attended = jnp.einsum(
        "nkgij,njkd->nikgd", weights, band_values, preferred_element_type=jnp.float32
    )
    return attended.astype(jnp.bfloat16).reshape(rows, kv_heads * group * HD)


def norm_rows(mid_rows, norm_gain):
    scale = lax.rsqrt(jnp.mean(mid_rows * mid_rows, axis=-1, keepdims=True) + 1e-06)
    return (mid_rows * scale * norm_gain).astype(jnp.bfloat16)


def by_place(pieces, me):
    for bit in bits_of(len(pieces)):
        flip = (me & bit) != 0
        pieces = [jnp.where(flip, pieces[r ^ bit], pieces[r]) for r in range(len(pieces))]
    return pieces


def own_rows(attended):
    count = lax.axis_size("tp")
    me = lax.axis_index("tp")
    rows = attended.shape[0] // count
    pieces = []
    for mask in range(count):
        piece = lax.dynamic_slice_in_dim(attended, (me ^ mask) * rows, rows)
        pieces.append(swapped(piece, "tp", mask) if mask else piece)
    return jnp.concatenate(by_place(pieces, me), axis=1)


def regrouped(gate_proj, up_proj, down_proj):
    me = lax.axis_index("sp") % SHARE
    width = gate_proj.shape[1] // SHARE
    gate_up, down = [], []
    for mask in range(SHARE):
        start = (me ^ mask) * width
        piece = jnp.concatenate(
            [
                lax.dynamic_slice_in_dim(gate_proj, start, width, axis=1),
                lax.dynamic_slice_in_dim(up_proj, start, width, axis=1),
            ],
            axis=1,
        )
        gate_up.append(swapped(piece, "sp", mask) if mask else piece)
    for mask in range(SHARE):
        piece = lax.dynamic_slice_in_dim(down_proj, (me ^ mask) * width, width, axis=0)
        down.append(swapped(piece, "sp", mask) if mask else piece)
    return (
        jnp.concatenate(by_place(gate_up, me), axis=0),
        jnp.concatenate(by_place(down, me), axis=1),
    )


def spread(chunk):
    groups = lax.axis_size("sp") // SHARE
    if groups == 4:
        half = chunk.shape[0] // 2
        low = swapped(chunk, "sp", SHARE)
        wrap = swapped(chunk, "sp", 3 * SHARE)
        first = swapped(low[:half], "sp", 3 * SHARE)
        second = swapped(wrap[half:], "sp", SHARE)
        return [chunk, low, jnp.concatenate([first, second], axis=0), wrap]
    chunks = [chunk]
    for bit in bits_of(groups):
        chunks = chunks + [swapped(piece, "sp", SHARE * bit) for piece in chunks]
    return chunks


def gathered(rows, hops):
    for axis, mask in hops:
        rows = jnp.concatenate([rows, swapped(rows, axis, mask)], axis=0)
    return rows


def scattered(partial, hops):
    total = partial
    for axis, mask in reversed(hops):
        half = total.shape[0] // 2
        arrived = swapped(total[half:].astype(jnp.bfloat16), axis, mask)
        total = total[:half].astype(jnp.float32) + arrived.astype(jnp.float32)
    return total


def shards(
    resid,
    queries,
    keys,
    values,
    documents,
    sinks,
    out_proj,
    norm_gain,
    gate_proj,
    up_proj,
    down_proj,
):
    groups = lax.axis_size("sp") // SHARE
    group = lax.axis_index("sp") // SHARE
    gate_up, down = regrouped(gate_proj, up_proj, down_proj)
    gate_up = jnp.concatenate(spread(gate_up), axis=0)
    down = jnp.concatenate(spread(down), axis=1)
    units = down.shape[0]

    attended = attend(queries, keys, values, documents, sinks)
    mid_rows = resid.astype(jnp.float32) + jnp.dot(
        own_rows(attended), out_proj, preferred_element_type=jnp.float32
    )
    normed = norm_rows(mid_rows, norm_gain)
    rows, width = normed.shape
    block = width // groups
    normed = jnp.concatenate(
        [lax.dynamic_slice_in_dim(normed, (group ^ k) * block, block, axis=1) for k in range(groups)],
        axis=1,
    )
    x_hops = [("tp", bit) for bit in bits_of(lax.axis_size("tp"))]
    y_hops = [("sp", 2)]
    core_hops = [("sp", 1)]
    sums = []
    for stream, hops in enumerate((x_hops + y_hops + core_hops, y_hops + x_hops + core_hops)):
        part = normed[stream * rows // 2 : (stream + 1) * rows // 2]
        part = gathered(part, hops)
        acts = jnp.dot(part, gate_up, preferred_element_type=jnp.float32)
        hidden = (jax.nn.silu(acts[:, :units]) * acts[:, units:]).astype(jnp.bfloat16)
        partial = jnp.dot(hidden, down, preferred_element_type=jnp.float32).astype(jnp.bfloat16)
        sums.append(scattered(partial, hops))
    summed = jnp.concatenate(sums, axis=0)
    stack = jnp.stack([summed[:, k * block : (k + 1) * block] for k in range(groups)])
    summed = jnp.concatenate(
        [lax.dynamic_index_in_dim(stack, group ^ k, keepdims=False) for k in range(groups)], axis=1
    )
    return (mid_rows + summed).astype(jnp.bfloat16)


MESH = pl.DeviceIdType.MESH
CHAIN, SIDE, CORES = 4, 2, 2


def fits(mesh):
    return mesh.shape["sp"] == CHAIN * SIDE * CORES and mesh.shape["tp"] == 2


def layer_kernel(
    documents_ref,
    gain_ref,
    sinks_ref,
    resid_hbm,
    queries_hbm,
    keys_hbm,
    values_hbm,
    out_proj_hbm,
    gate_hbm,
    up_hbm,
    down_hbm,
    out_ref,
    q_v,
    k_v,
    v_v,
    halo_docs,
    resid_v,
    out_proj_v,
    att,
    att_out,
    mid,
    tok,
    gu,
    dn,
    acts,
    hid,
    part,
    x_out,
    x_in,
    z_out,
    z_in,
    local_sem,
    halo_s,
    halo_r,
    own_s,
    own_r,
    tok_s,
    tok_r,
    wl,
    wz_s,
    wz_r,
    wy_s,
    wy_r,
    wc_s,
    wc_r,
    rx_s,
    rx_r,
    rz_s,
    rz_r,
):
    sp = lax.axis_index("sp")
    x = lax.axis_index("tp")
    z = sp // (SIDE * CORES)
    y = (sp // CORES) % SIDE
    c = sp % CORES
    hi, lo = z // 2, z % 2
    pair = z + 1 - 2 * lo
    far_mid = 2 - hi
    far_end = 3 - 3 * hi
    is_mid = jnp.where((z == 1) | (z == 2), 1, 0)

    def at(zz, yy, cc, xx):
        return ((zz * SIDE + yy) * CORES + cc, xx)

    to_pair, to_mid, to_end = at(pair, y, c, x), at(far_mid, y, c, x), at(far_end, y, c, x)
    to_y, to_c, to_x = at(z, 1 - y, c, x), at(z, y, 1 - c, x), (sp, 1 - x)
    count = CHAIN * SIDE * CORES
    to_next = (lax.rem(sp + 1, count), x)
    to_prev = (lax.rem(sp + count - 1, count), x)

    rows, own = q_v.shape[0], resid_v.shape[0]
    depth = gate_hbm.shape[0]
    units = gu.shape[2]
    width = mid.shape[1]
    heads = sinks_ref.shape[0]
    kv_heads = k_v.shape[1] // HD
    group = heads // kv_heads
    blocks = rows // WINDOW
    pane = dn.shape[2]
    cols = heads * HD

    def remote(src, dst, send, recv, device):
        return pltpu.make_async_remote_copy(
            src_ref=src, dst_ref=dst, send_sem=send, recv_sem=recv, device_id=device, device_id_type=MESH
        )

    fetch = [
        pltpu.make_async_copy(queries_hbm, q_v, local_sem.at[0]),
        pltpu.make_async_copy(keys_hbm, k_v.at[pl.ds(WINDOW, rows), :], local_sem.at[1]),
        pltpu.make_async_copy(values_hbm, v_v.at[pl.ds(WINDOW, rows), :], local_sem.at[2]),
        pltpu.make_async_copy(resid_hbm, resid_v, local_sem.at[3]),
        pltpu.make_async_copy(out_proj_hbm, out_proj_v, local_sem.at[4]),
    ]
    for copy in fetch:
        copy.start()

    barrier = pltpu.get_barrier_semaphore()
    around = (to_pair, to_mid, to_end, to_y, to_c, to_x, to_next, to_prev)
    for device in around:
        pl.semaphore_signal(barrier, inc=1, device_id=device, device_id_type=MESH)
    pl.semaphore_wait(barrier, len(around))

    last = pl.ds(rows - WINDOW, WINDOW)
    halo = [
        remote(keys_hbm.at[last, :], k_v.at[pl.ds(0, WINDOW), :], halo_s.at[0], halo_r.at[0], to_next),
        remote(values_hbm.at[last, :], v_v.at[pl.ds(0, WINDOW), :], halo_s.at[1], halo_r.at[1], to_next),
        remote(documents_ref.at[pl.ds(blocks - 1, 1), :], halo_docs, halo_s.at[2], halo_r.at[2], to_next),
    ]
    for copy in halo:
        copy.start()

    z_of = (z, pair, far_mid, far_end)

    def place(kind, zz, yy, cc):
        if kind == 2:
            return dn.at[zz * SIDE + yy, :, pl.ds(pl.multiple_of(cc * depth, depth), depth)]
        source = (zz * SIDE + yy) * CORES + cc
        return gu.at[kind, pl.ds(pl.multiple_of(source * depth, depth), depth), :]

    def shard(kind, half):
        start = pl.ds(pl.multiple_of(half * units, WINDOW), units)
        if kind == 2:
            return down_hbm.at[start, :]
        return (gate_hbm, up_hbm)[kind].at[:, start]

    def z_send(kind, dest):
        half, device, slot = (
            (1 - lo, to_pair, 0),
            (hi, to_mid, 2 - is_mid),
            (1 - hi, to_end, 2 - is_mid),
        )[dest]
        return remote(
            shard(kind, half), place(kind, z, y, c), wz_s.at[dest, kind], wz_r.at[slot, kind], device
        )

    def z_arrival(kind, slot):
        where = place(kind, z_of[slot], y, c)
        return remote(where, where, wz_s.at[slot - 1, kind], wz_r.at[slot - 1, kind], to_pair)

    def y_send(kind, slot):
        where = place(kind, z_of[slot], y, c)
        return remote(
            shard(kind, lo) if slot == 0 else where, where, wy_s.at[slot, kind], wy_r.at[slot, kind], to_y
        )

    def y_arrival(kind, slot):
        where = place(kind, z_of[slot], 1 - y, c)
        return remote(where, where, wy_s.at[slot, kind], wy_r.at[slot, kind], to_y)

    def c_send(kind, slot, other):
        where = place(kind, z_of[slot], 1 - y if other else y, c)
        source = shard(kind, lo) if slot == 0 and not other else where
        return remote(source, where, wc_s.at[slot, other, kind], wc_r.at[slot, other, kind], to_c)

    def c_arrival(kind, slot, other):
        where = place(kind, z_of[slot], 1 - y if other else y, 1 - c)
        return remote(where, where, wc_s.at[slot, other, kind], wc_r.at[slot, other, kind], to_c)

    kept = [
        pltpu.make_async_copy(shard(kind, lo), place(kind, z, y, c), wl.at[kind]) for kind in range(3)
    ]

    def z_in_and_on(kind, slot):
        z_arrival(kind, slot).wait_recv()
        y_send(kind, slot).start()
        c_send(kind, slot, 0).start()

    def y_in_and_on(kind, slot):
        y_arrival(kind, slot).wait_recv()
        c_send(kind, slot, 1).start()

    for kind in (0, 1):
        z_send(kind, 0).start()
        y_send(kind, 0).start()
        c_send(kind, 0, 0).start()
    y_send(2, 0).start()
    c_send(2, 0, 0).start()

    @pl.when(is_mid == 1)
    def _():
        for kind in (0, 1):
            z_send(kind, 1).start()
            z_send(kind, 2).start()

    for copy in kept:
        copy.start()

    for copy in fetch[:3]:
        copy.wait()
    for copy in halo:
        copy.wait_recv()

    row = lax.broadcasted_iota(jnp.int32, (WINDOW, 2 * WINDOW), 0)
    col = lax.broadcasted_iota(jnp.int32, (WINDOW, 2 * WINDOW), 1)
    distance = row + WINDOW - col
    in_window = (distance >= 0) & (distance < WINDOW)

    def attend_block(block, target, target_row, target_col):
        here = documents_ref[pl.ds(block, 1), :]
        back = documents_ref[pl.ds(jnp.maximum(block - 1, 0), 1), :]
        back = jnp.where(block == 0, halo_docs[...], back)
        band = jnp.concatenate([back, here], axis=1).astype(jnp.float32)
        mine = jnp.broadcast_to(here.astype(jnp.float32), (WINDOW, WINDOW)).T
        mine = jnp.concatenate([mine, mine], axis=1)
        first = jnp.where((sp == 0) & (block == 0), WINDOW, 0)
        visible = in_window & (band == mine) & (col >= first)
        start = pl.multiple_of(block * WINDOW, WINDOW)
        for kv in range(kv_heads):
            k_band = k_v[pl.ds(start, 2 * WINDOW), kv * HD : (kv + 1) * HD]
            v_band = v_v[pl.ds(start, 2 * WINDOW), kv * HD : (kv + 1) * HD]
            pieces = []
            for head in range(kv * group, (kv + 1) * group):
                q = q_v[pl.ds(start, WINDOW), head * HD : (head + 1) * HD]
                scores = lax.dot_general(
                    q, k_band, (((1,), (1,)), ((), ())), preferred_element_type=jnp.float32
                ) * HD ** (-0.5)
                scores = jnp.where(visible, scores, -jnp.inf)
                sink = sinks_ref[head]
                top = jnp.maximum(jnp.max(scores, axis=1, keepdims=True), sink)
                raw = jnp.exp(scores - top)
                total = jnp.sum(raw, axis=1, keepdims=True) + jnp.exp(sink - top)
                weights = (raw / total).astype(jnp.bfloat16)
                pieces.append(jnp.dot(weights, v_band, preferred_element_type=jnp.float32))
            merged = jnp.concatenate(pieces, axis=1).astype(jnp.bfloat16)
            at_col = target_col + kv * group * HD
            if not isinstance(at_col, int):
                at_col = pl.multiple_of(at_col, WINDOW)
            target[pl.ds(target_row, WINDOW), pl.ds(at_col, group * HD)] = merged

    own_blocks = own // WINDOW
    my_cols = pl.ds(pl.multiple_of(x * cols, WINDOW), cols)

    def own_send(part_index):
        part_rows = pl.ds(part_index * WINDOW, WINDOW)
        return remote(
            att_out.at[part_rows, :],
            att.at[part_rows, my_cols],
            own_s.at[part_index],
            own_r.at[part_index],
            to_x,
        )

    for b in range(own_blocks):
        attend_block((1 - x) * own_blocks + b, att_out, b * WINDOW, 0)
        own_send(b).start()
    for b in range(own_blocks):
        attend_block(x * own_blocks + b, att, b * WINDOW, x * cols)

    their_cols = pl.ds(pl.multiple_of((1 - x) * cols, WINDOW), cols)
    for copy in fetch[3:]:
        copy.wait()
    for b in range(own_blocks):
        where = att.at[pl.ds(b * WINDOW, WINDOW), their_cols]
        remote(where, where, own_s.at[b], own_r.at[b], to_x).wait_recv()

    square = jnp.zeros((own, 1), jnp.float32)
    step = 2 * pane
    for n in range(width // step):
        block_cols = pl.ds(n * step, step)
        value = resid_v[:, block_cols].astype(jnp.float32) + jnp.dot(
            att[...], out_proj_v[:, block_cols], preferred_element_type=jnp.float32
        )
        mid[:, block_cols] = value
        square = square + jnp.sum(value * value, axis=1, keepdims=True)
    scale = lax.rsqrt(square * (1.0 / width) + 1e-06)
    for n in range(width // step):
        block_cols = pl.ds(n * step, step)
        tok[pl.ds(0, own), block_cols] = (mid[:, block_cols] * scale * gain_ref[:, block_cols]).astype(
            jnp.bfloat16
        )

    def tok_at(slot):
        return tok.at[pl.ds(slot * own, own), :]

    tok_z = remote(tok_at(0), tok_at(1), tok_s.at[0], tok_r.at[0], to_pair)
    tok_x = remote(tok_at(0), tok_at(2), tok_s.at[1], tok_r.at[1], to_x)
    tok_on = remote(tok_at(1), tok_at(3), tok_s.at[2], tok_r.at[2], to_x)
    tok_z.start()
    tok_x.start()

    @pl.when(is_mid == 0)
    def _():
        for kind in (0, 1, 2):
            z_send(kind, 2).start()
            z_send(kind, 1).start()
        z_send(2, 0).start()

    def ready(kind, slot):
        c_arrival(kind, slot, 0).wait_recv()
        c_arrival(kind, slot, 1).wait_recv()

    tall = own * 4

    def gate_up(slot, first, final):
        deep = pl.ds(pl.multiple_of(z_of[slot] * SIDE * CORES * depth, depth), SIDE * CORES * depth)

        def tile(start, size):
            at_units = pl.ds(start, size)
            sums = []
            for kind in (0, 1):
                value = jnp.dot(tok[:, deep], gu[kind, deep, at_units], preferred_element_type=jnp.float32)
                if not first:
                    value = value + acts[kind, :, at_units]
                if not final:
                    acts[kind, :, at_units] = value
                sums.append(value)
            if final:
                gate_acts, up_acts = sums
                hid[:, at_units] = (gate_acts / (1.0 + jnp.exp(-gate_acts)) * up_acts).astype(jnp.bfloat16)

        whole = units // pane

        def body(n, carry):
            tile(pl.multiple_of(n * pane, pane), pane)
            return carry

        lax.fori_loop(0, whole, body, 0)
        if units % pane:
            tile(whole * pane, units % pane)

    z_in_and_on(0, 1)
    z_in_and_on(1, 1)
    y_in_and_on(0, 0)
    y_in_and_on(1, 0)
    y_in_and_on(2, 0)
    y_in_and_on(0, 1)
    tok_z.wait_recv()
    tok_on.start()
    y_in_and_on(1, 1)
    z_in_and_on(0, 2)
    z_in_and_on(1, 2)
    y_in_and_on(0, 2)
    tok_x.wait_recv()
    tok_on.wait_recv()
    kept[0].wait()
    kept[1].wait()
    ready(0, 0)
    ready(1, 0)
    gate_up(0, True, False)
    y_in_and_on(1, 2)
    z_in_and_on(0, 3)

    @pl.when(is_mid == 1)
    def _():
        for dest in (1, 2, 0):
            z_send(2, dest).start()

    ready(0, 1)
    ready(1, 1)
    gate_up(1, False, False)
    z_in_and_on(1, 3)
    ready(0, 2)
    ready(1, 2)
    gate_up(2, False, False)
    y_in_and_on(0, 3)
    z_in_and_on(2, 1)
    y_in_and_on(1, 3)
    ready(0, 3)
    ready(1, 3)
    gate_up(3, False, True)
    y_in_and_on(2, 1)
    kept[2].wait()

    half = tall // 2
    panes = [(slot, other) for slot in range(4) for other in range(2)]

    def pane_of(i):
        slot, other = panes[i]
        return z_of[slot] * SIDE + (1 - y if other else y)

    def x_sum(i):
        j = pane_of(i)
        return remote(x_out.at[j], x_in.at[j], rx_s.at[i], rx_r.at[i], to_x)

    def down_pane(i):
        j = pane_of(i)
        partial = jnp.dot(hid[...], dn[j], preferred_element_type=jnp.float32)
        x_out[j] = partial[half:, :].astype(jnp.bfloat16)
        part[j] = partial[:half, :]
        x_sum(i).start()

    def z_copy(j):
        return remote(z_out.at[j], z_in.at[j], rz_s.at[j], rz_r.at[j], to_pair)

    def fold(i):
        j = pane_of(i)
        x_sum(i).wait_recv()
        total = part[j] + x_in[j].astype(jnp.float32)
        z_out[j] = total[own:, :].astype(jnp.bfloat16)
        z_copy(j).start()
        part[j, pl.ds(0, own), :] = total[:own, :]

    def finish(i):
        j = pane_of(i)
        z_copy(j).wait_recv()
        at_cols = pl.ds(pl.multiple_of(j * pane, pane), pane)
        out_ref[:, at_cols] = (
            mid[:, at_cols] + (part[j, pl.ds(0, own), :] + z_in[j].astype(jnp.float32))
        ).astype(jnp.bfloat16)

    ready(2, 0)
    down_pane(0)
    down_pane(1)
    ready(2, 1)
    down_pane(2)
    down_pane(3)
    z_in_and_on(2, 2)
    fold(0)
    y_in_and_on(2, 2)
    fold(1)
    ready(2, 2)
    down_pane(4)
    down_pane(5)
    fold(2)
    z_in_and_on(2, 3)
    fold(3)
    y_in_and_on(2, 3)
    fold(4)
    ready(2, 3)
    down_pane(6)
    down_pane(7)
    fold(5)
    for i in range(4):
        finish(i)
    fold(6)
    fold(7)
    for i in range(4, 8):
        finish(i)

    for copy in halo:
        copy.wait_send()
    for b in range(own_blocks):
        own_send(b).wait_send()
    for copy in (tok_z, tok_x, tok_on):
        copy.wait_send()
    for kind in range(3):
        for dest in range(3):
            z_send(kind, dest).wait_send()
        for slot in range(4):
            y_send(kind, slot).wait_send()
            for other in range(2):
                c_send(kind, slot, other).wait_send()
    for i in range(8):
        x_sum(i).wait_send()
        z_copy(pane_of(i)).wait_send()


def one_kernel(
    resid, queries, keys, values, documents, sinks, out_proj, norm_gain, gate_proj, up_proj, down_proj
):
    rows, own, width = queries.shape[0], resid.shape[0], resid.shape[1]
    units = gate_proj.shape[1] // 2
    deep = gate_proj.shape[0] * CHAIN * SIDE * CORES
    pane = gate_proj.shape[0] * CORES
    panes = width // pane
    heads_cols, kv_cols = queries.shape[1], keys.shape[1]
    bf16, f32 = jnp.bfloat16, jnp.float32
    vmem = pl.BlockSpec(memory_space=pltpu.VMEM)
    anywhere = pl.BlockSpec(memory_space=pl.ANY)
    dma = pltpu.SemaphoreType.DMA
    tall = 4 * own
    return pl.pallas_call(
        layer_kernel,
        out_shape=jax.ShapeDtypeStruct((own, width), bf16),
        in_specs=[vmem, vmem, pl.BlockSpec(memory_space=pltpu.SMEM)] + [anywhere] * 8,
        out_specs=vmem,
        scratch_shapes=[
            pltpu.VMEM((rows, heads_cols), bf16),
            pltpu.VMEM((rows + WINDOW, kv_cols), bf16),
            pltpu.VMEM((rows + WINDOW, kv_cols), bf16),
            pltpu.VMEM((1, WINDOW), jnp.int32),
            pltpu.VMEM((own, width), bf16),
            pltpu.VMEM(out_proj.shape, bf16),
            pltpu.VMEM((own, out_proj.shape[0]), bf16),
            pltpu.VMEM((own, heads_cols), bf16),
            pltpu.VMEM((own, width), f32),
            pltpu.VMEM((tall, width), bf16),
            pltpu.VMEM((2, deep, units), bf16),
            pltpu.VMEM((panes, units, pane), bf16),
            pltpu.VMEM((2, tall, units), f32),
            pltpu.VMEM((tall, units), bf16),
            pltpu.VMEM((panes, tall // 2, pane), f32),
            pltpu.VMEM((panes, tall // 2, pane), bf16),
            pltpu.VMEM((panes, tall // 2, pane), bf16),
            pltpu.VMEM((panes, own, pane), bf16),
            pltpu.VMEM((panes, own, pane), bf16),
            dma((5,)),
            dma((3,)),
            dma((3,)),
            dma((own // WINDOW,)),
            dma((own // WINDOW,)),
            dma((3,)),
            dma((3,)),
            dma((3,)),
            dma((3, 3)),
            dma((3, 3)),
            dma((4, 3)),
            dma((4, 3)),
            dma((4, 2, 3)),
            dma((4, 2, 3)),
            dma((panes,)),
            dma((panes,)),
            dma((panes,)),
            dma((panes,)),
        ],
        compiler_params=pltpu.CompilerParams(
            collective_id=0, has_side_effects=True, vmem_limit_bytes=66_000_000
        ),
        name="layer",
    )(
        documents.reshape(rows // WINDOW, WINDOW),
        norm_gain.reshape(1, width),
        sinks,
        resid,
        queries,
        keys,
        values,
        out_proj,
        gate_proj,
        up_proj,
        down_proj,
    )


def solution(mesh):
    in_specs = (
        P(("sp", "tp"), None),
        P("sp", "tp"),
        P("sp", "tp"),
        P("sp", "tp"),
        P("sp"),
        P("tp"),
        P(),
        P(),
        P("sp", "tp"),
        P("sp", "tp"),
        P("tp", "sp"),
    )
    out_specs = P(("sp", "tp"), None)
    if fits(mesh):
        program = lambda *arrays: one_kernel(*arrays)
        return jax.shard_map(
            program, mesh=mesh, in_specs=in_specs, out_specs=out_specs, check_vma=False
        )
    return jax.shard_map(shards, mesh=mesh, in_specs=in_specs, out_specs=out_specs, check_vma=False)
```

profile of v0, /device:TPU:0, one launch (start us, length us, event | category | flops | bytes accessed | tf_op | source)
XLA Modules:
  0.0 185.9 jit_solution(8428873986937208346)
XLA Ops:
  0.0 183.6 %layer.1 = bf16[256,2048]{1,0:T(8,128)(2,1)} custom-call(s32[4,128]{1,0:T(4,128)} %bitcast.3, f32[1,2048]{1,0:T(1,128)} %bitcast.2, f32[8]{0:T(128)} %sinks_ref.1, bf16[256,2048]{1,0:T(8,128)(2,1)} %resid_hbm.1, bf16[512,512]{1,0:T(8,128)(2,1)} %queries_hbm.1, bf16[512,256]{1,0:T(8,128)(2,1)} %keys_hbm.1, bf16[512,256]{1,0:T(8,128)(2,1)} %values_hbm.1, ...), custom_call_target="tpu_custom_call" | custom-call | tf_op jit(solution)/shard_map/layer/pallas_call | solution.py:670
  183.6 2.3 %copy.13 = bf16[256,2048]{1,0:T(8,128)(2,1)} copy(bf16[256,2048]{1,0:T(8,128)(2,1)} %layer.1) | data formatting | bytes 2097152
where the time goes:
time: 186 us
  Pallas kernels  184 us (99%)
  local copies, waits for them, and re-layouts  2.3 us (1%)
    pallas_call x1, Pallas kernels, one_kernel(): pl.pallas_call(layer_kernel, out_shape=jax.ShapeDtypeStruct((own, width),...  184 us

commit v1 on v0

--- a/solution.py
+++ b/solution.py
@@ -317,51 +317,71 @@
     for copy in halo:
         copy.start()
 
-    z_of = (z, pair, far_mid, far_end)
+    mid_plane = is_mid == 1
+    rows_z = (z, jnp.where(mid_plane, far_end, pair), far_mid, jnp.where(mid_plane, pair, far_end))
+    cols_z = (
+        z,
+        jnp.where(mid_plane, far_mid, far_end),
+        jnp.where(mid_plane, pair, far_mid),
+        jnp.where(mid_plane, far_end, pair),
+    )
+    z_of = (rows_z, rows_z, cols_z, rows_z, rows_z, rows_z, rows_z)
+    row_slots = (
+        jnp.where(mid_plane, 1, 3),
+        jnp.where(mid_plane, 2, 1),
+        jnp.where(mid_plane, 2, 3),
+    )
+    col_slots = (
+        jnp.where(mid_plane, 3, 2),
+        jnp.where(mid_plane, 1, 3),
+        jnp.where(mid_plane, 2, 1),
+    )
+    upper, lower = (0, depth // 2), (depth // 2, depth // 2)
+    spans_of = ((0, depth), (0, depth), None, upper, lower, upper, lower)
+    array_of = (0, 1, 2, 1, 1, 0, 0)
+    late = (5, 6, 3, 4)
 
     def place(kind, zz, yy, cc):
         if kind == 2:
             return dn.at[zz * SIDE + yy, :, pl.ds(pl.multiple_of(cc * depth, depth), depth)]
         source = (zz * SIDE + yy) * CORES + cc
-        return gu.at[kind, pl.ds(pl.multiple_of(source * depth, depth), depth), :]
+        first, count = spans_of[kind]
+        return gu.at[array_of[kind], pl.ds(pl.multiple_of(source * depth + first, count), count), :]
 
     def shard(kind, half):
         start = pl.ds(pl.multiple_of(half * units, WINDOW), units)
         if kind == 2:
             return down_hbm.at[start, :]
-        return (gate_hbm, up_hbm)[kind].at[:, start]
+        return (gate_hbm, up_hbm)[array_of[kind]].at[pl.ds(*spans_of[kind]), start]
 
     def z_send(kind, dest):
-        half, device, slot = (
-            (1 - lo, to_pair, 0),
-            (hi, to_mid, 2 - is_mid),
-            (1 - hi, to_end, 2 - is_mid),
-        )[dest]
+        half, device = ((1 - lo, to_pair), (hi, to_mid), (1 - hi, to_end))[dest]
+        slot = (col_slots if kind == 2 else row_slots)[dest]
         return remote(
-            shard(kind, half), place(kind, z, y, c), wz_s.at[dest, kind], wz_r.at[slot, kind], device
+            shard(kind, half), place(kind, z, y, c), wz_s.at[dest, kind], wz_r.at[slot - 1, kind], device
         )
 
     def z_arrival(kind, slot):
-        where = place(kind, z_of[slot], y, c)
+        where = place(kind, z_of[kind][slot], y, c)
         return remote(where, where, wz_s.at[slot - 1, kind], wz_r.at[slot - 1, kind], to_pair)
 
     def y_send(kind, slot):
-        where = place(kind, z_of[slot], y, c)
+        where = place(kind, z_of[kind][slot], y, c)
         return remote(
             shard(kind, lo) if slot == 0 else where, where, wy_s.at[slot, kind], wy_r.at[slot, kind], to_y
         )
 
     def y_arrival(kind, slot):
-        where = place(kind, z_of[slot], 1 - y, c)
+        where = place(kind, z_of[kind][slot], 1 - y, c)
         return remote(where, where, wy_s.at[slot, kind], wy_r.at[slot, kind], to_y)
 
     def c_send(kind, slot, other):
-        where = place(kind, z_of[slot], 1 - y if other else y, c)
+        where = place(kind, z_of[kind][slot], 1 - y if other else y, c)
         source = shard(kind, lo) if slot == 0 and not other else where
         return remote(source, where, wc_s.at[slot, other, kind], wc_r.at[slot, other, kind], to_c)
 
     def c_arrival(kind, slot, other):
-        where = place(kind, z_of[slot], 1 - y if other else y, 1 - c)
+        where = place(kind, z_of[kind][slot], 1 - y if other else y, 1 - c)
         return remote(where, where, wc_s.at[slot, other, kind], wc_r.at[slot, other, kind], to_c)
 
     kept = [
@@ -377,41 +397,43 @@
         y_arrival(kind, slot).wait_recv()
         c_send(kind, slot, 1).start()
 
-    for kind in (0, 1):
-        z_send(kind, 0).start()
-        y_send(kind, 0).start()
-        c_send(kind, 0, 0).start()
-    y_send(2, 0).start()
-    c_send(2, 0, 0).start()
-
     @pl.when(is_mid == 1)
     def _():
         for kind in (0, 1):
+            z_send(kind, 0).start()
+
+    @pl.when(is_mid == 0)
+    def _():
+        for kind in (0, 1):
             z_send(kind, 1).start()
-            z_send(kind, 2).start()
+
+    for kind in (0, 1):
+        y_send(kind, 0).start()
+        c_send(kind, 0, 0).start()
+    c_send(2, 0, 0).start()
 
     for copy in kept:
         copy.start()
 
     for copy in fetch[:3]:
         copy.wait()
-    for copy in halo:
-        copy.wait_recv()
 
     row = lax.broadcasted_iota(jnp.int32, (WINDOW, 2 * WINDOW), 0)
     col = lax.broadcasted_iota(jnp.int32, (WINDOW, 2 * WINDOW), 1)
     distance = row + WINDOW - col
     in_window = (distance >= 0) & (distance < WINDOW)
 
-    def attend_block(block, target, target_row, target_col):
+    def attend_block(block, target, target_row, target_col, may_be_first):
         here = documents_ref[pl.ds(block, 1), :]
         back = documents_ref[pl.ds(jnp.maximum(block - 1, 0), 1), :]
-        back = jnp.where(block == 0, halo_docs[...], back)
+        if may_be_first:
+            back = jnp.where(block == 0, halo_docs[...], back)
         band = jnp.concatenate([back, here], axis=1).astype(jnp.float32)
         mine = jnp.broadcast_to(here.astype(jnp.float32), (WINDOW, WINDOW)).T
         mine = jnp.concatenate([mine, mine], axis=1)
-        first = jnp.where((sp == 0) & (block == 0), WINDOW, 0)
-        visible = in_window & (band == mine) & (col >= first)
+        visible = in_window & (band == mine)
+        if may_be_first:
+            visible = visible & (col >= jnp.where((sp == 0) & (block == 0), WINDOW, 0))
         start = pl.multiple_of(block * WINDOW, WINDOW)
         for kv in range(kv_heads):
             k_band = k_v[pl.ds(start, 2 * WINDOW), kv * HD : (kv + 1) * HD]
@@ -448,50 +470,70 @@
             to_x,
         )
 
-    for b in range(own_blocks):
-        attend_block((1 - x) * own_blocks + b, att_out, b * WINDOW, 0)
+    for b in reversed(range(own_blocks)):
+        if b == 0:
+            for copy in halo:
+                copy.wait_recv()
+        attend_block((1 - x) * own_blocks + b, att_out, b * WINDOW, 0, b == 0)
         own_send(b).start()
-    for b in range(own_blocks):
-        attend_block(x * own_blocks + b, att, b * WINDOW, x * cols)
+        attend_block(x * own_blocks + b, att, b * WINDOW, x * cols, b == 0)
 
     their_cols = pl.ds(pl.multiple_of((1 - x) * cols, WINDOW), cols)
+
     for copy in fetch[3:]:
         copy.wait()
+    square = jnp.zeros((own, 1), jnp.float32)
+    step = 2 * pane
+    my_rows = pl.ds(pl.multiple_of(x * cols, WINDOW), cols)
+    their_rows = pl.ds(pl.multiple_of((1 - x) * cols, WINDOW), cols)
+    for n in range(width // step):
+        block_cols = pl.ds(n * step, step)
+        mid[:, block_cols] = resid_v[:, block_cols].astype(jnp.float32) + jnp.dot(
+            att[:, my_cols], out_proj_v[my_rows, block_cols], preferred_element_type=jnp.float32
+        )
     for b in range(own_blocks):
         where = att.at[pl.ds(b * WINDOW, WINDOW), their_cols]
         remote(where, where, own_s.at[b], own_r.at[b], to_x).wait_recv()
-
-    square = jnp.zeros((own, 1), jnp.float32)
-    step = 2 * pane
     for n in range(width // step):
         block_cols = pl.ds(n * step, step)
-        value = resid_v[:, block_cols].astype(jnp.float32) + jnp.dot(
-            att[...], out_proj_v[:, block_cols], preferred_element_type=jnp.float32
+        value = mid[:, block_cols] + jnp.dot(
+            att[:, their_cols], out_proj_v[their_rows, block_cols], preferred_element_type=jnp.float32
         )
         mid[:, block_cols] = value
         square = square + jnp.sum(value * value, axis=1, keepdims=True)
     scale = lax.rsqrt(square * (1.0 / width) + 1e-06)
     for n in range(width // step):
         block_cols = pl.ds(n * step, step)
-        tok[pl.ds(0, own), block_cols] = (mid[:, block_cols] * scale * gain_ref[:, block_cols]).astype(
-            jnp.bfloat16
-        )
-
-    def tok_at(slot):
-        return tok.at[pl.ds(slot * own, own), :]
-
-    tok_z = remote(tok_at(0), tok_at(1), tok_s.at[0], tok_r.at[0], to_pair)
-    tok_x = remote(tok_at(0), tok_at(2), tok_s.at[1], tok_r.at[1], to_x)
-    tok_on = remote(tok_at(1), tok_at(3), tok_s.at[2], tok_r.at[2], to_x)
-    tok_z.start()
-    tok_x.start()
+        tok[pl.ds(0, own), block_cols] = (
+            mid[:, block_cols] * scale * gain_ref[:, block_cols]
+        ).astype(jnp.bfloat16)
+
+    bits = own // 2
+
+    def tok_at(slot, bit):
+        return tok.at[pl.ds(slot * own + bit * bits, bits), :]
+
+    tok_z = [remote(tok_at(0, i), tok_at(3, i), tok_s.at[0, i], tok_r.at[0, i], to_pair) for i in range(2)]
+    tok_x = [remote(tok_at(0, i), tok_at(1, i), tok_s.at[1, i], tok_r.at[1, i], to_x) for i in range(2)]
+    tok_on = [remote(tok_at(3, i), tok_at(2, i), tok_s.at[2, i], tok_r.at[2, i], to_x) for i in range(2)]
+    for i in range(2):
+        tok_z[i].start()
+        tok_x[i].start()
+
+    @pl.when(is_mid == 1)
+    def _():
+        for dest in (2, 1):
+            for kind in (0, 1):
+                z_send(kind, dest).start()
+        z_send(2, 1).start()
 
     @pl.when(is_mid == 0)
     def _():
-        for kind in (0, 1, 2):
-            z_send(kind, 2).start()
-            z_send(kind, 1).start()
-        z_send(2, 0).start()
+        for dest in (0, 2):
+            for kind in late:
+                z_send(kind, dest).start()
+        for dest in (2, 0, 1):
+            z_send(2, dest).start()
 
     def ready(kind, slot):
         c_arrival(kind, slot, 0).wait_recv()
@@ -499,22 +541,27 @@
 
     tall = own * 4
 
-    def gate_up(slot, first, final):
-        deep = pl.ds(pl.multiple_of(z_of[slot] * SIDE * CORES * depth, depth), SIDE * CORES * depth)
+    def gate_up(slot, spans, first=False, final=None, kinds=(0, 1)):
+        source = z_of[0][slot] * (SIDE * CORES * depth)
+        deep = pl.ds(pl.multiple_of(source, SIDE * CORES * depth), SIDE * CORES * depth)
 
         def tile(start, size):
             at_units = pl.ds(start, size)
-            sums = []
-            for kind in (0, 1):
-                value = jnp.dot(tok[:, deep], gu[kind, deep, at_units], preferred_element_type=jnp.float32)
-                if not first:
-                    value = value + acts[kind, :, at_units]
-                if not final:
-                    acts[kind, :, at_units] = value
-                sums.append(value)
-            if final:
-                gate_acts, up_acts = sums
-                hid[:, at_units] = (gate_acts / (1.0 + jnp.exp(-gate_acts)) * up_acts).astype(jnp.bfloat16)
+            for position, (at_row, height) in enumerate(spans):
+                span = pl.ds(at_row, height)
+                for kind in kinds:
+                    value = jnp.dot(
+                        tok[span, deep], gu[kind, deep, at_units], preferred_element_type=jnp.float32
+                    )
+                    if not first:
+                        value = value + acts[kind, span, at_units]
+                    if final is None:
+                        acts[kind, span, at_units] = value
+                if final is not None:
+                    gate_acts = acts[0, span, at_units]
+                    hid[pl.ds(final + position * height, height), at_units] = (
+                        gate_acts / (1.0 + jnp.exp(-gate_acts)) * value
+                    ).astype(jnp.bfloat16)
 
         whole = units // pane
 
@@ -526,131 +573,253 @@
         if units % pane:
             tile(whole * pane, units % pane)
 
-    z_in_and_on(0, 1)
-    z_in_and_on(1, 1)
-    y_in_and_on(0, 0)
-    y_in_and_on(1, 0)
-    y_in_and_on(2, 0)
-    y_in_and_on(0, 1)
-    tok_z.wait_recv()
-    tok_on.start()
-    y_in_and_on(1, 1)
-    z_in_and_on(0, 2)
-    z_in_and_on(1, 2)
-    y_in_and_on(0, 2)
-    tok_x.wait_recv()
-    tok_on.wait_recv()
-    kept[0].wait()
-    kept[1].wait()
-    ready(0, 0)
-    ready(1, 0)
-    gate_up(0, True, False)
-    y_in_and_on(1, 2)
-    z_in_and_on(0, 3)
-
-    @pl.when(is_mid == 1)
-    def _():
-        for dest in (1, 2, 0):
-            z_send(2, dest).start()
-
-    ready(0, 1)
-    ready(1, 1)
-    gate_up(1, False, False)
-    z_in_and_on(1, 3)
-    ready(0, 2)
-    ready(1, 2)
-    gate_up(2, False, False)
-    y_in_and_on(0, 3)
-    z_in_and_on(2, 1)
-    y_in_and_on(1, 3)
-    ready(0, 3)
-    ready(1, 3)
-    gate_up(3, False, True)
-    y_in_and_on(2, 1)
-    kept[2].wait()
+    def gate_only(slot):
+        gate_up(slot, near, kinds=(0,))
+        gate_up(slot, far, kinds=(0,))
+
+    def last_up(slot, spans, final):
+        gate_up(slot, spans, final=final, kinds=(1,))
 
     half = tall // 2
+    near, theirs, paired = ((0, half),), ((half, own),), ((half + own, own),)
+    far = ((half, half),)
+    sent, held = ((own, half),), ((0, own), (tall - own, own))
+
     panes = [(slot, other) for slot in range(4) for other in range(2)]
+    pair_first = ()
 
     def pane_of(i):
         slot, other = panes[i]
-        return z_of[slot] * SIDE + (1 - y if other else y)
+        return z_of[2][slot] * SIDE + (1 - y if other else y)
 
     def x_sum(i):
         j = pane_of(i)
-        return remote(x_out.at[j], x_in.at[j], rx_s.at[i], rx_r.at[i], to_x)
-
-    def down_pane(i):
+        device = to_pair if i in pair_first else to_x
+        return remote(x_out.at[j], x_in.at[j], rx_s.at[i], rx_r.at[i], device)
+
+    def z_sum(i):
         j = pane_of(i)
-        partial = jnp.dot(hid[...], dn[j], preferred_element_type=jnp.float32)
-        x_out[j] = partial[half:, :].astype(jnp.bfloat16)
-        part[j] = partial[:half, :]
+        device = to_x if i in pair_first else to_pair
+        return remote(z_out.at[j], z_in.at[j], rz_s.at[j], rz_r.at[j], device)
+
+    def down_sent(i):
+        j = pane_of(i)
+        x_out[j] = jnp.dot(
+            hid[pl.ds(0, half), :], dn[j], preferred_element_type=jnp.float32
+        ).astype(jnp.bfloat16)
         x_sum(i).start()
 
-    def z_copy(j):
-        return remote(z_out.at[j], z_in.at[j], rz_s.at[j], rz_r.at[j], to_pair)
+    def down_held(i):
+        j = pane_of(i)
+        part[j] = jnp.dot(hid[pl.ds(half, half), :], dn[j], preferred_element_type=jnp.float32)
 
     def fold(i):
         j = pane_of(i)
         x_sum(i).wait_recv()
         total = part[j] + x_in[j].astype(jnp.float32)
         z_out[j] = total[own:, :].astype(jnp.bfloat16)
-        z_copy(j).start()
+        z_sum(i).start()
         part[j, pl.ds(0, own), :] = total[:own, :]
 
     def finish(i):
         j = pane_of(i)
-        z_copy(j).wait_recv()
+        z_sum(i).wait_recv()
         at_cols = pl.ds(pl.multiple_of(j * pane, pane), pane)
         out_ref[:, at_cols] = (
             mid[:, at_cols] + (part[j, pl.ds(0, own), :] + z_in[j].astype(jnp.float32))
         ).astype(jnp.bfloat16)
 
-    ready(2, 0)
-    down_pane(0)
-    down_pane(1)
-    ready(2, 1)
-    down_pane(2)
-    down_pane(3)
-    z_in_and_on(2, 2)
-    fold(0)
-    y_in_and_on(2, 2)
-    fold(1)
-    ready(2, 2)
-    down_pane(4)
-    down_pane(5)
-    fold(2)
-    z_in_and_on(2, 3)
-    fold(3)
-    y_in_and_on(2, 3)
-    fold(4)
-    ready(2, 3)
-    down_pane(6)
-    down_pane(7)
-    fold(5)
-    for i in range(4):
-        finish(i)
-    fold(6)
-    fold(7)
-    for i in range(4, 8):
-        finish(i)
+    def tok_forward(i):
+        tok_z[i].wait_recv()
+        tok_on[i].start()
+
+    def tok_wait(group):
+        for copy in group:
+            copy.wait_recv()
+
+    def late_down(dest):
+        z_send(2, dest).start()
+
+    def own_down():
+        y_send(2, 0).start()
+
+    def apart(ends, mids):
+        for want, listed in ((0, ends), (1, mids)):
+
+            @pl.when(is_mid == want)
+            def _():
+                run(listed)
+
+    def kept_wait(kind):
+        kept[kind].wait()
+
+    steps = (
+        (y_in_and_on, 0, 0),
+        (z_in_and_on, 0, 1),
+        (y_in_and_on, 1, 0),
+        (z_in_and_on, 1, 1),
+        (y_in_and_on, 0, 1),
+        (
+            apart,
+            ((z_in_and_on, 0, 2), (y_in_and_on, 1, 1), (z_in_and_on, 1, 2)),
+            ((tok_forward, 0), (y_in_and_on, 1, 1), (own_down,), (tok_forward, 1)),
+        ),
+        (tok_wait, tok_x),
+        (kept_wait, 0),
+        (kept_wait, 1),
+        (ready, 0, 0),
+        (ready, 1, 0),
+        (gate_up, 0, near, True),
+        (ready, 0, 1),
+        (ready, 1, 1),
+        (gate_up, 1, near),
+        (
+            apart,
+            (
+                (y_in_and_on, 0, 2),
+                (tok_forward, 0),
+                (own_down,),
+                (y_in_and_on, 1, 2),
+                (tok_forward, 1),
+            ),
+            ((z_in_and_on, 0, 2), (z_in_and_on, 5, 3), (z_in_and_on, 6, 3), (z_in_and_on, 1, 2)),
+        ),
+        (gate_up, 0, paired, True),
+        (apart, ((z_in_and_on, 5, 3),), ((z_in_and_on, 3, 3), (y_in_and_on, 0, 2))),
+        (gate_up, 1, paired),
+        (
+            apart,
+            (
+                (ready, 0, 2),
+                (ready, 1, 2),
+                (gate_up, 2, near),
+                (z_in_and_on, 6, 3),
+                (gate_up, 2, paired),
+                (z_in_and_on, 3, 3),
+            ),
+            ((z_in_and_on, 4, 3), (y_in_and_on, 5, 3)),
+        ),
+        (tok_wait, tok_on),
+        (gate_up, 0, theirs, True),
+        (
+            apart,
+            ((z_in_and_on, 4, 3), (y_in_and_on, 5, 3), (y_in_and_on, 6, 3)),
+            ((y_in_and_on, 6, 3),),
+        ),
+        (gate_up, 1, theirs),
+        (
+            apart,
+            (),
+            (
+                (y_in_and_on, 1, 2),
+                (ready, 0, 2),
+                (ready, 1, 2),
+                (gate_up, 2, near),
+                (gate_up, 2, paired),
+                (late_down, 2),
+            ),
+        ),
+        (gate_up, 2, theirs),
+        (y_in_and_on, 2, 0),
+        (y_in_and_on, 3, 3),
+        (ready, 5, 3),
+        (ready, 6, 3),
+        (gate_only, 3),
+        (y_in_and_on, 4, 3),
+        (apart, (), ((late_down, 0),)),
+        (z_in_and_on, 2, 1),
+        (ready, 3, 3),
+        (ready, 4, 3),
+        (last_up, 3, sent, 0),
+        (kept_wait, 2),
+        (ready, 2, 0),
+        (down_sent, 0),
+        (down_sent, 1),
+        (last_up, 3, held, half),
+        (down_held, 0),
+        (y_in_and_on, 2, 1),
+        (z_in_and_on, 2, 2),
+        (fold, 0),
+        (ready, 2, 1),
+        (down_sent, 2),
+        (down_sent, 3),
+        (down_held, 1),
+        (fold, 1),
+        (z_in_and_on, 2, 3),
+        (y_in_and_on, 2, 2),
+        (down_held, 2),
+        (ready, 2, 2),
+        (down_sent, 4),
+        (down_sent, 5),
+        (fold, 2),
+        (down_held, 3),
+        (y_in_and_on, 2, 3),
+        (ready, 2, 3),
+        (down_sent, 6),
+        (down_sent, 7),
+        (fold, 3),
+        (down_held, 4),
+        (fold, 4),
+        (down_held, 5),
+        (fold, 5),
+        (down_held, 6),
+        (down_held, 7),
+        (fold, 6),
+        (fold, 7),
+        (finish, 0),
+        (finish, 1),
+        (finish, 2),
+        (finish, 3),
+        (finish, 4),
+        (finish, 5),
+        (finish, 6),
+        (finish, 7),
+    )
+
+    def run(listed):
+        for action, *given in listed:
+            if action is apart:
+                apart(*given)
+                continue
+            action(*given)
+
+    run(steps)
 
     for copy in halo:
         copy.wait_send()
     for b in range(own_blocks):
         own_send(b).wait_send()
-    for copy in (tok_z, tok_x, tok_on):
+    for copy in tok_z + tok_x + tok_on:
         copy.wait_send()
-    for kind in range(3):
-        for dest in range(3):
-            z_send(kind, dest).wait_send()
-        for slot in range(4):
+    for kind in (0, 1, 2):
+        for slot in range(3):
             y_send(kind, slot).wait_send()
             for other in range(2):
                 c_send(kind, slot, other).wait_send()
+    for kind in (2,) + late:
+        y_send(kind, 3).wait_send()
+        for other in range(2):
+            c_send(kind, 3, other).wait_send()
+    for dest in range(3):
+        z_send(2, dest).wait_send()
+
+    @pl.when(is_mid == 1)
+    def _():
+        for kind in (0, 1):
+            for dest in range(3):
+                z_send(kind, dest).wait_send()
+
+    @pl.when(is_mid == 0)
+    def _():
+        for kind in (0, 1):
+            z_send(kind, 1).wait_send()
+        for kind in late:
+            z_send(kind, 0).wait_send()
+            z_send(kind, 2).wait_send()
+
     for i in range(8):
         x_sum(i).wait_send()
-        z_copy(pane_of(i)).wait_send()
+        z_sum(i).wait_send()
 
 
 def one_kernel(
@@ -697,15 +866,15 @@
             dma((3,)),
             dma((own // WINDOW,)),
             dma((own // WINDOW,)),
+            dma((3, 2)),
+            dma((3, 2)),
             dma((3,)),
-            dma((3,)),
-            dma((3,)),
-            dma((3, 3)),
-            dma((3, 3)),
-            dma((4, 3)),
-            dma((4, 3)),
-            dma((4, 2, 3)),
-            dma((4, 2, 3)),
+            dma((3, 7)),
+            dma((3, 7)),
+            dma((4, 7)),
+            dma((4, 7)),
+            dma((4, 2, 7)),
+            dma((4, 2, 7)),
             dma((panes,)),
             dma((panes,)),
             dma((panes,)),

time: 186 us -> 152 us (0.82)
  Pallas kernels: 184 us -> 149 us
    pallas_call x1, Pallas kernels: 184 us -> 149 us  [one_kernel(): pl.pallas_call(layer_kernel, out_shape=jax.ShapeDtypeStruct((own, width),...]
where the time goes in v1:
time: 152 us
  Pallas kernels  149 us (98%)
  local copies, waits for them, and re-layouts  2.3 us (2%)
    pallas_call x1, Pallas kernels, one_kernel(): pl.pallas_call(layer_kernel, out_shape=jax.ShapeDtypeStruct((own, width),...  149 us

profile of v1, /device:TPU:0, one launch (start us, length us, event | category | flops | bytes accessed | tf_op | source)
XLA Modules:
  0.0 151.6 jit_solution(11062617628022715172)
XLA Ops:
  0.0 149.3 %layer.1 = bf16[256,2048]{1,0:T(8,128)(2,1)} custom-call(s32[4,128]{1,0:T(4,128)} %bitcast.3, f32[1,2048]{1,0:T(1,128)} %bitcast.2, f32[8]{0:T(128)} %sinks_ref.1, bf16[256,2048]{1,0:T(8,128)(2,1)} %resid_hbm.1, bf16[512,512]{1,0:T(8,128)(2,1)} %queries_hbm.1, bf16[512,256]{1,0:T(8,128)(2,1)} %keys_hbm.1, bf16[512,256]{1,0:T(8,128)(2,1)} %values_hbm.1, ...), custom_call_target="tpu_custom_call" | custom-call | tf_op jit(solution)/shard_map/layer/pallas_call | solution.py:839
  149.3 2.3 %copy.13 = bf16[256,2048]{1,0:T(8,128)(2,1)} copy(bf16[256,2048]{1,0:T(8,128)(2,1)} %layer.1) | data formatting | bytes 2097152

commit v2 on v1

--- a/solution.py
+++ b/solution.py
@@ -218,6 +218,7 @@
     up_hbm,
     down_hbm,
     out_ref,
+    out_v,
     q_v,
     k_v,
     v_v,
@@ -255,6 +256,7 @@
     rx_r,
     rz_s,
     rz_r,
+    out_sem,
 ):
     sp = lax.axis_index("sp")
     x = lax.axis_index("tp")
@@ -319,23 +321,14 @@
 
     mid_plane = is_mid == 1
     rows_z = (z, jnp.where(mid_plane, far_end, pair), far_mid, jnp.where(mid_plane, pair, far_end))
-    cols_z = (
-        z,
-        jnp.where(mid_plane, far_mid, far_end),
-        jnp.where(mid_plane, pair, far_mid),
-        jnp.where(mid_plane, far_end, pair),
-    )
+    cols_z = (z, far_mid, pair, far_end)
     z_of = (rows_z, rows_z, cols_z, rows_z, rows_z, rows_z, rows_z)
     row_slots = (
         jnp.where(mid_plane, 1, 3),
         jnp.where(mid_plane, 2, 1),
         jnp.where(mid_plane, 2, 3),
     )
-    col_slots = (
-        jnp.where(mid_plane, 3, 2),
-        jnp.where(mid_plane, 1, 3),
-        jnp.where(mid_plane, 2, 1),
-    )
+    col_slots = (2, jnp.where(mid_plane, 1, 3), jnp.where(mid_plane, 1, 3))
     upper, lower = (0, depth // 2), (depth // 2, depth // 2)
     spans_of = ((0, depth), (0, depth), None, upper, lower, upper, lower)
     array_of = (0, 1, 2, 1, 1, 0, 0)
@@ -532,8 +525,7 @@
         for dest in (0, 2):
             for kind in late:
                 z_send(kind, dest).start()
-        for dest in (2, 0, 1):
-            z_send(2, dest).start()
+        z_send(2, 0).start()
 
     def ready(kind, slot):
         c_arrival(kind, slot, 0).wait_recv()
@@ -592,12 +584,17 @@
         slot, other = panes[i]
         return z_of[2][slot] * SIDE + (1 - y if other else y)
 
-    def x_sum(i):
+    whole_rows = {0: pl.ds(0, own), 1: pl.ds(own, own)}
+
+    def first_hop(i, relayed):
         j = pane_of(i)
         device = to_pair if i in pair_first else to_x
-        return remote(x_out.at[j], x_in.at[j], rx_s.at[i], rx_r.at[i], device)
-
-    def z_sum(i):
+        taken = whole_rows[relayed]
+        return remote(
+            x_out.at[j, taken, :], x_in.at[j, taken, :], rx_s.at[i, relayed], rx_r.at[i, relayed], device
+        )
+
+    def second_hop(i):
         j = pane_of(i)
         device = to_x if i in pair_first else to_pair
         return remote(z_out.at[j], z_in.at[j], rz_s.at[j], rz_r.at[j], device)
@@ -607,27 +604,38 @@
         x_out[j] = jnp.dot(
             hid[pl.ds(0, half), :], dn[j], preferred_element_type=jnp.float32
         ).astype(jnp.bfloat16)
-        x_sum(i).start()
+        first_hop(i, 1).start()
 
     def down_held(i):
         j = pane_of(i)
         part[j] = jnp.dot(hid[pl.ds(half, half), :], dn[j], preferred_element_type=jnp.float32)
 
-    def fold(i):
+    def send_rest(*given):
+        for i in given:
+            first_hop(i, 0).start()
+
+    def relay(i):
         j = pane_of(i)
-        x_sum(i).wait_recv()
-        total = part[j] + x_in[j].astype(jnp.float32)
-        z_out[j] = total[own:, :].astype(jnp.bfloat16)
-        z_sum(i).start()
-        part[j, pl.ds(0, own), :] = total[:own, :]
+        first_hop(i, 1).wait_recv()
+        z_out[j] = (part[j, whole_rows[1], :] + x_in[j, whole_rows[1], :].astype(jnp.float32)).astype(
+            jnp.bfloat16
+        )
+        second_hop(i).start()
+
+    def store(i):
+        at_cols = pl.ds(pl.multiple_of(pane_of(i) * pane, pane), pane)
+        return pltpu.make_async_copy(out_v.at[:, at_cols], out_ref.at[:, at_cols], out_sem.at[i])
 
     def finish(i):
         j = pane_of(i)
-        z_sum(i).wait_recv()
+        first_hop(i, 0).wait_recv()
+        second_hop(i).wait_recv()
         at_cols = pl.ds(pl.multiple_of(j * pane, pane), pane)
-        out_ref[:, at_cols] = (
-            mid[:, at_cols] + (part[j, pl.ds(0, own), :] + z_in[j].astype(jnp.float32))
-        ).astype(jnp.bfloat16)
+        summed = part[j, whole_rows[0], :] + x_in[j, whole_rows[0], :].astype(jnp.float32)
+        out_v[:, at_cols] = (mid[:, at_cols] + (summed + z_in[j].astype(jnp.float32))).astype(
+            jnp.bfloat16
+        )
+        store(i).start()
 
     def tok_forward(i):
         tok_z[i].wait_recv()
@@ -652,6 +660,39 @@
 
     def kept_wait(kind):
         kept[kind].wait()
+
+    def settle():
+        for copy in halo:
+            copy.wait_send()
+        for b in range(own_blocks):
+            own_send(b).wait_send()
+        for copy in tok_z + tok_x + tok_on:
+            copy.wait_send()
+        for kind in (0, 1, 2):
+            for slot in range(3):
+                y_send(kind, slot).wait_send()
+                for other in range(2):
+                    c_send(kind, slot, other).wait_send()
+        for kind in (2,) + late:
+            y_send(kind, 3).wait_send()
+            for other in range(2):
+                c_send(kind, 3, other).wait_send()
+        for dest in range(3):
+            z_send(2, dest).wait_send()
+
+        @pl.when(is_mid == 1)
+        def _():
+            for kind in (0, 1):
+                for dest in range(3):
+                    z_send(kind, dest).wait_send()
+
+        @pl.when(is_mid == 0)
+        def _():
+            for kind in (0, 1):
+                z_send(kind, 1).wait_send()
+            for kind in late:
+                z_send(kind, 0).wait_send()
+                z_send(kind, 2).wait_send()
 
     steps = (
         (y_in_and_on, 0, 0),
@@ -701,71 +742,85 @@
         ),
         (tok_wait, tok_on),
         (gate_up, 0, theirs, True),
-        (
-            apart,
-            ((z_in_and_on, 4, 3), (y_in_and_on, 5, 3), (y_in_and_on, 6, 3)),
-            ((y_in_and_on, 6, 3),),
-        ),
+        (apart, (), ((y_in_and_on, 6, 3),)),
         (gate_up, 1, theirs),
         (
             apart,
-            (),
             (
+                (z_in_and_on, 4, 3),
+                (y_in_and_on, 5, 3),
+                (y_in_and_on, 6, 3),
+                (gate_up, 2, theirs),
+                (ready, 5, 3),
+                (ready, 6, 3),
+                (gate_only, 3),
+            ),
+            (
+                (late_down, 2),
+                (ready, 5, 3),
+                (ready, 6, 3),
+                (gate_only, 3),
                 (y_in_and_on, 1, 2),
+                (y_in_and_on, 2, 0),
+                (late_down, 0),
                 (ready, 0, 2),
                 (ready, 1, 2),
                 (gate_up, 2, near),
-                (gate_up, 2, paired),
-                (late_down, 2),
+                (y_in_and_on, 3, 3),
+                (gate_up, 2, far),
             ),
         ),
-        (gate_up, 2, theirs),
-        (y_in_and_on, 2, 0),
-        (y_in_and_on, 3, 3),
-        (ready, 5, 3),
-        (ready, 6, 3),
-        (gate_only, 3),
+        (apart, ((y_in_and_on, 2, 0), (y_in_and_on, 3, 3)), ()),
         (y_in_and_on, 4, 3),
-        (apart, (), ((late_down, 0),)),
-        (z_in_and_on, 2, 1),
         (ready, 3, 3),
         (ready, 4, 3),
         (last_up, 3, sent, 0),
         (kept_wait, 2),
         (ready, 2, 0),
         (down_sent, 0),
+        (apart, ((late_down, 1), (late_down, 2)), ()),
+        (z_in_and_on, 2, 1),
+        (send_rest, 0),
         (down_sent, 1),
+        (send_rest, 1),
         (last_up, 3, held, half),
+        (z_in_and_on, 2, 2),
         (down_held, 0),
         (y_in_and_on, 2, 1),
-        (z_in_and_on, 2, 2),
-        (fold, 0),
+        (down_held, 1),
         (ready, 2, 1),
         (down_sent, 2),
+        (send_rest, 2),
+        (apart, (), ((z_in_and_on, 2, 3),)),
         (down_sent, 3),
-        (down_held, 1),
-        (fold, 1),
-        (z_in_and_on, 2, 3),
+        (send_rest, 3),
+        (relay, 0),
+        (relay, 1),
         (y_in_and_on, 2, 2),
         (down_held, 2),
         (ready, 2, 2),
         (down_sent, 4),
+        (send_rest, 4),
         (down_sent, 5),
-        (fold, 2),
+        (send_rest, 5),
+        (apart, ((z_in_and_on, 2, 3),), ()),
         (down_held, 3),
+        (relay, 2),
+        (relay, 3),
         (y_in_and_on, 2, 3),
         (ready, 2, 3),
         (down_sent, 6),
         (down_sent, 7),
-        (fold, 3),
+        (send_rest, 6, 7),
         (down_held, 4),
-        (fold, 4),
+        (relay, 4),
         (down_held, 5),
-        (fold, 5),
         (down_held, 6),
+        (relay, 5),
         (down_held, 7),
-        (fold, 6),
-        (fold, 7),
+        (settle,),
+        (relay, 6),
+        (relay, 7),
         (finish, 0),
         (finish, 1),
         (finish, 2),
@@ -785,41 +840,12 @@
 
     run(steps)
 
-    for copy in halo:
-        copy.wait_send()
-    for b in range(own_blocks):
-        own_send(b).wait_send()
-    for copy in tok_z + tok_x + tok_on:
-        copy.wait_send()
-    for kind in (0, 1, 2):
-        for slot in range(3):
-            y_send(kind, slot).wait_send()
-            for other in range(2):
-                c_send(kind, slot, other).wait_send()
-    for kind in (2,) + late:
-        y_send(kind, 3).wait_send()
-        for other in range(2):
-            c_send(kind, 3, other).wait_send()
-    for dest in range(3):
-        z_send(2, dest).wait_send()
-
-    @pl.when(is_mid == 1)
-    def _():
-        for kind in (0, 1):
-            for dest in range(3):
-                z_send(kind, dest).wait_send()
-
-    @pl.when(is_mid == 0)
-    def _():
-        for kind in (0, 1):
-            z_send(kind, 1).wait_send()
-        for kind in late:
-            z_send(kind, 0).wait_send()
-            z_send(kind, 2).wait_send()
-
-    for i in range(8):
-        x_sum(i).wait_send()
-        z_sum(i).wait_send()
+    for i in range(len(panes)):
+        first_hop(i, 0).wait_send()
+        first_hop(i, 1).wait_send()
+        second_hop(i).wait_send()
+    for i in range(len(panes)):
+        store(i).wait()
 
 
 def one_kernel(
@@ -840,8 +866,9 @@
         layer_kernel,
         out_shape=jax.ShapeDtypeStruct((own, width), bf16),
         in_specs=[vmem, vmem, pl.BlockSpec(memory_space=pltpu.SMEM)] + [anywhere] * 8,
-        out_specs=vmem,
+        out_specs=anywhere,
         scratch_shapes=[
+            pltpu.VMEM((own, width), bf16),
             pltpu.VMEM((rows, heads_cols), bf16),
             pltpu.VMEM((rows + WINDOW, kv_cols), bf16),
             pltpu.VMEM((rows + WINDOW, kv_cols), bf16),
@@ -875,7 +902,8 @@
             dma((4, 7)),
             dma((4, 2, 7)),
             dma((4, 2, 7)),
-            dma((panes,)),
+            dma((panes, 2)),
+            dma((panes, 2)),
             dma((panes,)),
             dma((panes,)),
             dma((panes,)),

time: 152 us -> 144 us (0.947)
  Pallas kernels: 149 us -> 141 us
    pallas_call x1, Pallas kernels: 149 us -> 141 us  [one_kernel(): pl.pallas_call(layer_kernel, out_shape=jax.ShapeDtypeStruct((own, width),...]
where the time goes in v2:
time: 144 us
  Pallas kernels  141 us (98%)
  local copies, waits for them, and re-layouts  2.3 us (2%)
    pallas_call x1, Pallas kernels, one_kernel(): pl.pallas_call(layer_kernel, out_shape=jax.ShapeDtypeStruct((own, width),...  141 us

profile of v2, /device:TPU:0, one launch (start us, length us, event | category | flops | bytes accessed | tf_op | source)
XLA Modules:
  0.0 143.7 jit_solution(590574350335448059)
XLA Ops:
  0.0 141.3 %layer.1 = bf16[256,2048]{1,0:T(8,128)(2,1)} custom-call(s32[4,128]{1,0:T(4,128)} %bitcast.3, f32[1,2048]{1,0:T(1,128)} %bitcast.2, f32[8]{0:T(128)} %sinks_ref.1, bf16[256,2048]{1,0:T(8,128)(2,1)} %resid_hbm.1, bf16[512,512]{1,0:T(8,128)(2,1)} %queries_hbm.1, bf16[512,256]{1,0:T(8,128)(2,1)} %keys_hbm.1, bf16[512,256]{1,0:T(8,128)(2,1)} %values_hbm.1, ...), custom_call_target="tpu_custom_call" | custom-call | tf_op jit(solution)/shard_map/layer/pallas_call | solution.py:865
  141.3 2.3 %copy.13 = bf16[256,2048]{1,0:T(8,128)(2,1)} copy(bf16[256,2048]{1,0:T(8,128)(2,1)} %layer.1) | data formatting | bytes 2097152

commit v3 on v2

--- a/solution.py
+++ b/solution.py
@@ -322,17 +322,26 @@
     mid_plane = is_mid == 1
     rows_z = (z, jnp.where(mid_plane, far_end, pair), far_mid, jnp.where(mid_plane, pair, far_end))
     cols_z = (z, far_mid, pair, far_end)
-    z_of = (rows_z, rows_z, cols_z, rows_z, rows_z, rows_z, rows_z)
+    z_of = (rows_z, rows_z, cols_z) + (rows_z,) * 8
     row_slots = (
         jnp.where(mid_plane, 1, 3),
         jnp.where(mid_plane, 2, 1),
         jnp.where(mid_plane, 2, 3),
     )
     col_slots = (2, jnp.where(mid_plane, 1, 3), jnp.where(mid_plane, 1, 3))
-    upper, lower = (0, depth // 2), (depth // 2, depth // 2)
-    spans_of = ((0, depth), (0, depth), None, upper, lower, upper, lower)
-    array_of = (0, 1, 2, 1, 1, 0, 0)
-    late = (5, 6, 3, 4)
+    quarters = tuple((q * depth // 4, depth // 4) for q in range(4))
+    spans_of = ((0, depth), (0, depth), None) + quarters + quarters
+    array_of = (0, 1, 2) + (0,) * 4 + (1,) * 4
+    late = tuple(range(3, 11))
+
+    def z_flag(kind, slot):
+        return kind + 4 if kind > 2 else 3 + slot if kind == 2 else 2 * (slot - 1) + kind
+
+    def y_flag(kind, slot):
+        return kind + 7 if kind > 2 else 6 + slot if kind == 2 else 2 * slot + kind
+
+    def c_flag(kind, slot):
+        return 3 + (kind > 6) if kind > 2 else 5 + slot if kind == 2 else slot
 
     def place(kind, zz, yy, cc):
         if kind == 2:
@@ -351,31 +360,27 @@
         half, device = ((1 - lo, to_pair), (hi, to_mid), (1 - hi, to_end))[dest]
         slot = (col_slots if kind == 2 else row_slots)[dest]
         return remote(
-            shard(kind, half), place(kind, z, y, c), wz_s.at[dest, kind], wz_r.at[slot - 1, kind], device
+            shard(kind, half), place(kind, z, y, c), wz_s.at[0], wz_r.at[z_flag(kind, slot)], device
         )
 
     def z_arrival(kind, slot):
         where = place(kind, z_of[kind][slot], y, c)
-        return remote(where, where, wz_s.at[slot - 1, kind], wz_r.at[slot - 1, kind], to_pair)
+        return remote(where, where, wz_s.at[0], wz_r.at[z_flag(kind, slot)], to_pair)
 
     def y_send(kind, slot):
         where = place(kind, z_of[kind][slot], y, c)
         return remote(
-            shard(kind, lo) if slot == 0 else where, where, wy_s.at[slot, kind], wy_r.at[slot, kind], to_y
+            shard(kind, lo) if slot == 0 else where, where, wy_s.at[0], wy_r.at[y_flag(kind, slot)], to_y
         )
 
     def y_arrival(kind, slot):
         where = place(kind, z_of[kind][slot], 1 - y, c)
-        return remote(where, where, wy_s.at[slot, kind], wy_r.at[slot, kind], to_y)
+        return remote(where, where, wy_s.at[0], wy_r.at[y_flag(kind, slot)], to_y)
 
     def c_send(kind, slot, other):
         where = place(kind, z_of[kind][slot], 1 - y if other else y, c)
         source = shard(kind, lo) if slot == 0 and not other else where
-        return remote(source, where, wc_s.at[slot, other, kind], wc_r.at[slot, other, kind], to_c)
-
-    def c_arrival(kind, slot, other):
-        where = place(kind, z_of[kind][slot], 1 - y if other else y, 1 - c)
-        return remote(where, where, wc_s.at[slot, other, kind], wc_r.at[slot, other, kind], to_c)
+        return remote(source, where, wc_s.at[0], wc_r.at[c_flag(kind, slot)], to_c)
 
     kept = [
         pltpu.make_async_copy(shard(kind, lo), place(kind, z, y, c), wl.at[kind]) for kind in range(3)
@@ -458,7 +463,7 @@
         return remote(
             att_out.at[part_rows, :],
             att.at[part_rows, my_cols],
-            own_s.at[part_index],
+            own_s.at[0],
             own_r.at[part_index],
             to_x,
         )
@@ -486,7 +491,7 @@
         )
     for b in range(own_blocks):
         where = att.at[pl.ds(b * WINDOW, WINDOW), their_cols]
-        remote(where, where, own_s.at[b], own_r.at[b], to_x).wait_recv()
+        remote(where, where, own_s.at[0], own_r.at[b], to_x).wait_recv()
     for n in range(width // step):
         block_cols = pl.ds(n * step, step)
         value = mid[:, block_cols] + jnp.dot(
@@ -506,9 +511,9 @@
     def tok_at(slot, bit):
         return tok.at[pl.ds(slot * own + bit * bits, bits), :]
 
-    tok_z = [remote(tok_at(0, i), tok_at(3, i), tok_s.at[0, i], tok_r.at[0, i], to_pair) for i in range(2)]
-    tok_x = [remote(tok_at(0, i), tok_at(1, i), tok_s.at[1, i], tok_r.at[1, i], to_x) for i in range(2)]
-    tok_on = [remote(tok_at(3, i), tok_at(2, i), tok_s.at[2, i], tok_r.at[2, i], to_x) for i in range(2)]
+    tok_z = [remote(tok_at(0, i), tok_at(3, i), tok_s.at[0], tok_r.at[0, i], to_pair) for i in range(2)]
+    tok_x = [remote(tok_at(0, i), tok_at(1, i), tok_s.at[0], tok_r.at[1, i], to_x) for i in range(2)]
+    tok_on = [remote(tok_at(3, i), tok_at(2, i), tok_s.at[0], tok_r.at[2, i], to_x) for i in range(2)]
     for i in range(2):
         tok_z[i].start()
         tok_x[i].start()
@@ -527,9 +532,20 @@
                 z_send(kind, dest).start()
         z_send(2, 0).start()
 
-    def ready(kind, slot):
-        c_arrival(kind, slot, 0).wait_recv()
-        c_arrival(kind, slot, 1).wait_recv()
+    def landed(where, semaphore):
+        remote(where, where, wc_s.at[0], semaphore, to_c).wait_recv()
+
+    def ready_rows(slot):
+        landed(gu.at[:, pl.ds(0, 2 * depth), :], wc_r.at[slot])
+
+    def ready_gate():
+        landed(gu.at[0, pl.ds(0, 2 * depth), :], wc_r.at[3])
+
+    def ready_up():
+        landed(gu.at[1, pl.ds(0, 2 * depth), :], wc_r.at[4])
+
+    def ready_down(slot):
+        landed(dn.at[0], wc_r.at[5 + slot])
 
     tall = own * 4
 
@@ -541,6 +557,7 @@
             at_units = pl.ds(start, size)
             for position, (at_row, height) in enumerate(spans):
                 span = pl.ds(at_row, height)
+                sums = []
                 for kind in kinds:
                     value = jnp.dot(
                         tok[span, deep], gu[kind, deep, at_units], preferred_element_type=jnp.float32
@@ -549,8 +566,9 @@
                         value = value + acts[kind, span, at_units]
                     if final is None:
                         acts[kind, span, at_units] = value
+                    sums.append(value)
                 if final is not None:
-                    gate_acts = acts[0, span, at_units]
+                    gate_acts = sums[0] if len(kinds) == 2 else acts[0, span, at_units]
                     hid[pl.ds(final + position * height, height), at_units] = (
                         gate_acts / (1.0 + jnp.exp(-gate_acts)) * value
                     ).astype(jnp.bfloat16)
@@ -566,8 +584,7 @@
             tile(whole * pane, units % pane)
 
     def gate_only(slot):
-        gate_up(slot, near, kinds=(0,))
-        gate_up(slot, far, kinds=(0,))
+        gate_up(slot, sent, kinds=(0,))
 
     def last_up(slot, spans, final):
         gate_up(slot, spans, final=final, kinds=(1,))
@@ -578,7 +595,7 @@
     sent, held = ((own, half),), ((0, own), (tall - own, own))
 
     panes = [(slot, other) for slot in range(4) for other in range(2)]
-    pair_first = ()
+    pair_first = (3,)
 
     def pane_of(i):
         slot, other = panes[i]
@@ -591,13 +608,13 @@
         device = to_pair if i in pair_first else to_x
         taken = whole_rows[relayed]
         return remote(
-            x_out.at[j, taken, :], x_in.at[j, taken, :], rx_s.at[i, relayed], rx_r.at[i, relayed], device
+            x_out.at[j, taken, :], x_in.at[j, taken, :], rx_s.at[0], rx_r.at[i, relayed], device
         )
 
     def second_hop(i):
         j = pane_of(i)
         device = to_x if i in pair_first else to_pair
-        return remote(z_out.at[j], z_in.at[j], rz_s.at[j], rz_r.at[j], device)
+        return remote(z_out.at[j], z_in.at[j], rz_s.at[0], rz_r.at[j], device)
 
     def down_sent(i):
         j = pane_of(i)
@@ -610,6 +627,15 @@
         j = pane_of(i)
         part[j] = jnp.dot(hid[pl.ds(half, half), :], dn[j], preferred_element_type=jnp.float32)
 
+    def down_both(i):
+        j = pane_of(i)
+        partial = jnp.dot(hid[...], dn[j], preferred_element_type=jnp.float32)
+        x_out[j, whole_rows[0], :] = partial[3 * own :, :].astype(jnp.bfloat16)
+        x_out[j, whole_rows[1], :] = partial[own : 2 * own, :].astype(jnp.bfloat16)
+        first_hop(i, 1).start()
+        part[j, whole_rows[0], :] = partial[2 * own : 3 * own, :]
+        part[j, whole_rows[1], :] = partial[:own, :]
+
     def send_rest(*given):
         for i in given:
             first_hop(i, 0).start()
@@ -624,7 +650,7 @@
 
     def store(i):
         at_cols = pl.ds(pl.multiple_of(pane_of(i) * pane, pane), pane)
-        return pltpu.make_async_copy(out_v.at[:, at_cols], out_ref.at[:, at_cols], out_sem.at[i])
+        return pltpu.make_async_copy(out_v.at[:, at_cols], out_ref.at[:, at_cols], out_sem.at[0])
 
     def finish(i):
         j = pane_of(i)
@@ -664,35 +690,22 @@
     def settle():
         for copy in halo:
             copy.wait_send()
-        for b in range(own_blocks):
-            own_send(b).wait_send()
-        for copy in tok_z + tok_x + tok_on:
-            copy.wait_send()
-        for kind in (0, 1, 2):
-            for slot in range(3):
-                y_send(kind, slot).wait_send()
-                for other in range(2):
-                    c_send(kind, slot, other).wait_send()
-        for kind in (2,) + late:
-            y_send(kind, 3).wait_send()
-            for other in range(2):
-                c_send(kind, 3, other).wait_send()
-        for dest in range(3):
-            z_send(2, dest).wait_send()
-
-        @pl.when(is_mid == 1)
-        def _():
-            for kind in (0, 1):
-                for dest in range(3):
-                    z_send(kind, dest).wait_send()
-
-        @pl.when(is_mid == 0)
-        def _():
-            for kind in (0, 1):
-                z_send(kind, 1).wait_send()
-            for kind in late:
-                z_send(kind, 0).wait_send()
-                z_send(kind, 2).wait_send()
+        for where, semaphore in (
+            (att_out, own_s),
+            (tok.at[pl.ds(0, 3 * own), :], tok_s),
+            (gu.at[0, pl.ds(0, 9 * depth), :], wz_s),
+            (gu.at[0, pl.ds(0, 12 * depth), :], wy_s),
+            (gu.at[:, pl.ds(0, 12 * depth), :], wc_s),
+        ):
+            remote(where, where, semaphore.at[0], halo_r.at[0], to_x).wait_send()
+
+    def z_late(*kinds):
+        for kind in kinds:
+            z_in_and_on(kind, 3)
+
+    def y_late(*kinds):
+        for kind in kinds:
+            y_in_and_on(kind, 3)
 
     steps = (
         (y_in_and_on, 0, 0),
@@ -703,16 +716,15 @@
         (
             apart,
             ((z_in_and_on, 0, 2), (y_in_and_on, 1, 1), (z_in_and_on, 1, 2)),
-            ((tok_forward, 0), (y_in_and_on, 1, 1), (own_down,), (tok_forward, 1)),
+            ((tok_forward, 0), (y_in_and_on, 1, 1), (own_down,), (tok_forward, 1), (z_in_and_on, 0, 2)),
         ),
         (tok_wait, tok_x),
         (kept_wait, 0),
         (kept_wait, 1),
-        (ready, 0, 0),
-        (ready, 1, 0),
+        (ready_rows, 0),
         (gate_up, 0, near, True),
-        (ready, 0, 1),
-        (ready, 1, 1),
+        (apart, (), ((z_late, 3, 4),)),
+        (ready_rows, 1),
         (gate_up, 1, near),
         (
             apart,
@@ -723,92 +735,76 @@
                 (y_in_and_on, 1, 2),
                 (tok_forward, 1),
             ),
-            ((z_in_and_on, 0, 2), (z_in_and_on, 5, 3), (z_in_and_on, 6, 3), (z_in_and_on, 1, 2)),
+            ((z_late, 5, 6), (z_in_and_on, 1, 2)),
         ),
         (gate_up, 0, paired, True),
-        (apart, ((z_in_and_on, 5, 3),), ((z_in_and_on, 3, 3), (y_in_and_on, 0, 2))),
+        (
+            apart,
+            ((ready_rows, 2), (gate_up, 2, near), (z_late, 3, 4)),
+            ((z_late, 7, 8), (y_in_and_on, 0, 2)),
+        ),
         (gate_up, 1, paired),
         (
             apart,
-            (
-                (ready, 0, 2),
-                (ready, 1, 2),
-                (gate_up, 2, near),
-                (z_in_and_on, 6, 3),
-                (gate_up, 2, paired),
-                (z_in_and_on, 3, 3),
-            ),
-            ((z_in_and_on, 4, 3), (y_in_and_on, 5, 3)),
+            ((z_late, 5), (gate_up, 2, paired), (z_late, 6, 7)),
+            ((z_late, 9, 10), (y_late, 3, 4)),
         ),
         (tok_wait, tok_on),
         (gate_up, 0, theirs, True),
-        (apart, (), ((y_in_and_on, 6, 3),)),
+        (apart, ((z_late, 8), (y_late, 3, 4)), ((y_late, 5, 6),)),
         (gate_up, 1, theirs),
         (
             apart,
-            (
-                (z_in_and_on, 4, 3),
-                (y_in_and_on, 5, 3),
-                (y_in_and_on, 6, 3),
-                (gate_up, 2, theirs),
-                (ready, 5, 3),
-                (ready, 6, 3),
-                (gate_only, 3),
-            ),
+            ((z_late, 9), (y_late, 5, 6), (z_late, 10), (gate_up, 2, theirs), (ready_gate,), (gate_only, 3)),
             (
                 (late_down, 2),
-                (ready, 5, 3),
-                (ready, 6, 3),
+                (y_in_and_on, 1, 2),
+                (ready_gate,),
                 (gate_only, 3),
-                (y_in_and_on, 1, 2),
-                (y_in_and_on, 2, 0),
+                (ready_rows, 2),
+                (gate_up, 2, near),
                 (late_down, 0),
-                (ready, 0, 2),
-                (ready, 1, 2),
-                (gate_up, 2, near),
-                (y_in_and_on, 3, 3),
+                (y_late, 7, 8),
                 (gate_up, 2, far),
             ),
         ),
-        (apart, ((y_in_and_on, 2, 0), (y_in_and_on, 3, 3)), ()),
-        (y_in_and_on, 4, 3),
-        (ready, 3, 3),
-        (ready, 4, 3),
+        (apart, ((y_late, 7, 8),), ()),
+        (y_in_and_on, 2, 0),
+        (y_late, 9, 10),
+        (ready_up,),
         (last_up, 3, sent, 0),
         (kept_wait, 2),
-        (ready, 2, 0),
+        (ready_down, 0),
         (down_sent, 0),
         (apart, ((late_down, 1), (late_down, 2)), ()),
         (z_in_and_on, 2, 1),
         (send_rest, 0),
         (down_sent, 1),
         (send_rest, 1),
-        (last_up, 3, held, half),
+        (gate_up, 3, held, False, half),
         (z_in_and_on, 2, 2),
         (down_held, 0),
         (y_in_and_on, 2, 1),
         (down_held, 1),
-        (ready, 2, 1),
+        (ready_down, 1),
         (down_sent, 2),
         (send_rest, 2),
-        (apart, (), ((z_in_and_on, 2, 3),)),
-        (down_sent, 3),
+        (down_both, 3),
         (send_rest, 3),
         (relay, 0),
         (relay, 1),
         (y_in_and_on, 2, 2),
-        (down_held, 2),
-        (ready, 2, 2),
+        (ready_down, 2),
         (down_sent, 4),
         (send_rest, 4),
+        (z_in_and_on, 2, 3),
         (down_sent, 5),
         (send_rest, 5),
-        (apart, ((z_in_and_on, 2, 3),), ()),
-        (down_held, 3),
+        (down_held, 2),
         (relay, 2),
         (relay, 3),
         (y_in_and_on, 2, 3),
-        (ready, 2, 3),
+        (ready_down, 3),
         (down_sent, 6),
         (down_sent, 7),
         (send_rest, 6, 7),
@@ -840,12 +836,9 @@
 
     run(steps)
 
-    for i in range(len(panes)):
-        first_hop(i, 0).wait_send()
-        first_hop(i, 1).wait_send()
-        second_hop(i).wait_send()
-    for i in range(len(panes)):
-        store(i).wait()
+    remote(x_out, x_out, rx_s.at[0], halo_r.at[0], to_x).wait_send()
+    remote(z_out, z_out, rz_s.at[0], halo_r.at[0], to_x).wait_send()
+    pltpu.make_async_copy(out_v, out_ref, out_sem.at[0]).wait()
 
 
 def one_kernel(
@@ -891,22 +884,22 @@
             dma((5,)),
             dma((3,)),
             dma((3,)),
+            dma((1,)),
             dma((own // WINDOW,)),
-            dma((own // WINDOW,)),
-            dma((3, 2)),
+            dma((1,)),
             dma((3, 2)),
             dma((3,)),
-            dma((3, 7)),
-            dma((3, 7)),
-            dma((4, 7)),
-            dma((4, 7)),
-            dma((4, 2, 7)),
-            dma((4, 2, 7)),
+            dma((1,)),
+            dma((15,)),
+            dma((1,)),
+            dma((18,)),
+            dma((1,)),
+            dma((9,)),
+            dma((1,)),
             dma((panes, 2)),
-            dma((panes, 2)),
+            dma((1,)),
             dma((panes,)),
-            dma((panes,)),
-            dma((panes,)),
+            dma((1,)),
         ],
         compiler_params=pltpu.CompilerParams(
             collective_id=0, has_side_effects=True, vmem_limit_bytes=66_000_000

time: 144 us -> 139 us (0.965)
  Pallas kernels: 141 us -> 135 us
    pallas_call x1, Pallas kernels: 141 us -> 135 us  [one_kernel(): pl.pallas_call(layer_kernel, out_shape=jax.ShapeDtypeStruct((own, width),...]
where the time goes in v3:
time: 139 us; the launch traced here: 138 us
  Pallas kernels  135 us (97%)
  local copies, waits for them, and re-layouts  2.3 us (2%)
    pallas_call x1, Pallas kernels, one_kernel(): pl.pallas_call(layer_kernel, out_shape=jax.ShapeDtypeStruct((own, width),...  135 us

profile of v3, /device:TPU:0, one launch (start us, length us, event | category | flops | bytes accessed | tf_op | source)
XLA Modules:
  0.0 137.6 jit_solution(12809703028230756054)
XLA Ops:
  0.0 135.3 %layer.1 = bf16[256,2048]{1,0:T(8,128)(2,1)} custom-call(s32[4,128]{1,0:T(4,128)} %bitcast.3, f32[1,2048]{1,0:T(1,128)} %bitcast.2, f32[8]{0:T(128)} %sinks_ref.1, bf16[256,2048]{1,0:T(8,128)(2,1)} %resid_hbm.1, bf16[512,512]{1,0:T(8,128)(2,1)} %queries_hbm.1, bf16[512,256]{1,0:T(8,128)(2,1)} %keys_hbm.1, bf16[512,256]{1,0:T(8,128)(2,1)} %values_hbm.1, ...), custom_call_target="tpu_custom_call" | custom-call | tf_op jit(solution)/shard_map/layer/pallas_call | solution.py:858
  135.3 2.3 %copy.13 = bf16[256,2048]{1,0:T(8,128)(2,1)} copy(bf16[256,2048]{1,0:T(8,128)(2,1)} %layer.1) | data formatting | bytes 2097152

commit v4 on v3

--- a/solution.py
+++ b/solution.py
@@ -206,9 +206,9 @@
 
 
 def layer_kernel(
-    documents_ref,
-    gain_ref,
-    sinks_ref,
+    documents_hbm,
+    gain_hbm,
+    sinks_hbm,
     resid_hbm,
     queries_hbm,
     keys_hbm,
@@ -218,6 +218,9 @@
     up_hbm,
     down_hbm,
     out_ref,
+    documents_ref,
+    gain_ref,
+    sinks_ref,
     out_v,
     q_v,
     k_v,
@@ -282,7 +285,7 @@
     depth = gate_hbm.shape[0]
     units = gu.shape[2]
     width = mid.shape[1]
-    heads = sinks_ref.shape[0]
+    heads = sinks_ref.shape[1]
     kv_heads = k_v.shape[1] // HD
     group = heads // kv_heads
     blocks = rows // WINDOW
@@ -294,6 +297,11 @@
             src_ref=src, dst_ref=dst, send_sem=send, recv_sem=recv, device_id=device, device_id_type=MESH
         )
 
+    small = [
+        pltpu.make_async_copy(documents_hbm, documents_ref, local_sem.at[5]),
+        pltpu.make_async_copy(gain_hbm, gain_ref, local_sem.at[6]),
+        pltpu.make_async_copy(sinks_hbm, sinks_ref, local_sem.at[7]),
+    ]
     fetch = [
         pltpu.make_async_copy(queries_hbm, q_v, local_sem.at[0]),
         pltpu.make_async_copy(keys_hbm, k_v.at[pl.ds(WINDOW, rows), :], local_sem.at[1]),
@@ -301,7 +309,7 @@
         pltpu.make_async_copy(resid_hbm, resid_v, local_sem.at[3]),
         pltpu.make_async_copy(out_proj_hbm, out_proj_v, local_sem.at[4]),
     ]
-    for copy in fetch:
+    for copy in small + fetch:
         copy.start()
 
     barrier = pltpu.get_barrier_semaphore()
@@ -316,6 +324,7 @@
         remote(values_hbm.at[last, :], v_v.at[pl.ds(0, WINDOW), :], halo_s.at[1], halo_r.at[1], to_next),
         remote(documents_ref.at[pl.ds(blocks - 1, 1), :], halo_docs, halo_s.at[2], halo_r.at[2], to_next),
     ]
+    small[0].wait()
     for copy in halo:
         copy.start()
 
@@ -413,7 +422,7 @@
     for copy in kept:
         copy.start()
 
-    for copy in fetch[:3]:
+    for copy in small[1:] + fetch[:3]:
         copy.wait()
 
     row = lax.broadcasted_iota(jnp.int32, (WINDOW, 2 * WINDOW), 0)
@@ -443,7 +452,7 @@
                     q, k_band, (((1,), (1,)), ((), ())), preferred_element_type=jnp.float32
                 ) * HD ** (-0.5)
                 scores = jnp.where(visible, scores, -jnp.inf)
-                sink = sinks_ref[head]
+                sink = sinks_ref[0, head]
                 top = jnp.maximum(jnp.max(scores, axis=1, keepdims=True), sink)
                 raw = jnp.exp(scores - top)
                 total = jnp.sum(raw, axis=1, keepdims=True) + jnp.exp(sink - top)
@@ -591,7 +600,7 @@
 
     half = tall // 2
     near, theirs, paired = ((0, half),), ((half, own),), ((half + own, own),)
-    far = ((half, half),)
+    far, direct = ((half, half),), ((own, own),)
     sent, held = ((own, half),), ((0, own), (tall - own, own))
 
     panes = [(slot, other) for slot in range(4) for other in range(2)]
@@ -622,6 +631,14 @@
             hid[pl.ds(0, half), :], dn[j], preferred_element_type=jnp.float32
         ).astype(jnp.bfloat16)
         first_hop(i, 1).start()
+
+    def down_half(i, relayed):
+        j = pane_of(i)
+        taken = whole_rows[relayed]
+        x_out[j, taken, :] = jnp.dot(
+            hid[taken, :], dn[j], preferred_element_type=jnp.float32
+        ).astype(jnp.bfloat16)
+        first_hop(i, relayed).start()
 
     def down_held(i):
         j = pane_of(i)
@@ -772,13 +789,14 @@
         (y_in_and_on, 2, 0),
         (y_late, 9, 10),
         (ready_up,),
-        (last_up, 3, sent, 0),
+        (z_in_and_on, 2, 1),
+        (last_up, 3, direct, 0),
+        (apart, ((late_down, 1), (late_down, 2)), ()),
         (kept_wait, 2),
         (ready_down, 0),
-        (down_sent, 0),
-        (apart, ((late_down, 1), (late_down, 2)), ()),
-        (z_in_and_on, 2, 1),
-        (send_rest, 0),
+        (down_half, 0, 0),
+        (last_up, 3, theirs, own),
+        (down_half, 0, 1),
         (down_sent, 1),
         (send_rest, 1),
         (gate_up, 3, held, False, half),
@@ -793,11 +811,12 @@
         (send_rest, 3),
         (relay, 0),
         (relay, 1),
+        (apart, (), ((z_in_and_on, 2, 3),)),
         (y_in_and_on, 2, 2),
         (ready_down, 2),
         (down_sent, 4),
         (send_rest, 4),
-        (z_in_and_on, 2, 3),
+        (apart, ((z_in_and_on, 2, 3),), ()),
         (down_sent, 5),
         (send_rest, 5),
         (down_held, 2),
@@ -851,16 +870,18 @@
     panes = width // pane
     heads_cols, kv_cols = queries.shape[1], keys.shape[1]
     bf16, f32 = jnp.bfloat16, jnp.float32
-    vmem = pl.BlockSpec(memory_space=pltpu.VMEM)
     anywhere = pl.BlockSpec(memory_space=pl.ANY)
     dma = pltpu.SemaphoreType.DMA
     tall = 4 * own
     return pl.pallas_call(
         layer_kernel,
         out_shape=jax.ShapeDtypeStruct((own, width), bf16),
-        in_specs=[vmem, vmem, pl.BlockSpec(memory_space=pltpu.SMEM)] + [anywhere] * 8,
+        in_specs=[anywhere] * 11,
         out_specs=anywhere,
         scratch_shapes=[
+            pltpu.VMEM((rows // WINDOW, WINDOW), jnp.int32),
+            pltpu.VMEM((1, width), f32),
+            pltpu.SMEM((1, sinks.shape[0]), f32),
             pltpu.VMEM((own, width), bf16),
             pltpu.VMEM((rows, heads_cols), bf16),
             pltpu.VMEM((rows + WINDOW, kv_cols), bf16),
@@ -881,7 +902,7 @@
             pltpu.VMEM((panes, tall // 2, pane), bf16),
             pltpu.VMEM((panes, own, pane), bf16),
             pltpu.VMEM((panes, own, pane), bf16),
-            dma((5,)),
+            dma((8,)),
             dma((3,)),
             dma((3,)),
             dma((1,)),
@@ -908,7 +929,7 @@
     )(
         documents.reshape(rows // WINDOW, WINDOW),
         norm_gain.reshape(1, width),
-        sinks,
+        sinks.reshape(1, sinks.shape[0]),
         resid,
         queries,
         keys,

time: 139 us -> 137 us (0.986)
  no operation moved by 1% of the time
where the time goes in v4:
time: 137 us
  Pallas kernels  134 us (98%)
  local copies, waits for them, and re-layouts  2.3 us (2%)
    pallas_call x1, Pallas kernels, one_kernel(): pl.pallas_call(layer_kernel, out_shape=jax.ShapeDtypeStruct((own, width),...  134 us

profile of v4, /device:TPU:0, one launch (start us, length us, event | category | flops | bytes accessed | tf_op | source)
XLA Modules:
  0.0 136.8 jit_solution(3044034526151997964)
XLA Ops:
  0.0 134.5 %layer.1 = bf16[256,2048]{1,0:T(8,128)(2,1)} custom-call(s32[4,128]{1,0:T(4,128)} %bitcast.4, f32[1,2048]{1,0:T(1,128)} %bitcast.3, f32[1,8]{1,0:T(1,128)} %bitcast.5, bf16[256,2048]{1,0:T(8,128)(2,1)} %resid_hbm.1, bf16[512,512]{1,0:T(8,128)(2,1)} %queries_hbm.1, bf16[512,256]{1,0:T(8,128)(2,1)} %keys_hbm.1, bf16[512,256]{1,0:T(8,128)(2,1)} %values_hbm.1, ...), custom_call_target="tpu_custom_call" | custom-call | tf_op jit(solution)/shard_map/layer/pallas_call | solution.py:876
  134.5 2.3 %copy.13 = bf16[256,2048]{1,0:T(8,128)(2,1)} copy(bf16[256,2048]{1,0:T(8,128)(2,1)} %layer.1) | data formatting | bytes 2097152
